TPU v7x, 32 devices: a whole 2x2x4 slice. The times are simulated.
32 devices in a mesh: ep: 8 (over z, x), tp: 4 (over y, core).
Axes of the slice: x: 2, y: 2, z: 4, core: 2. Of those that a mesh axis runs over, the one named last changes fastest.
Arguments:
- x_attend: bfloat16 [4096, 2048], P('ep'), may hold values from -6 to 6
- attend_gain: float32 [2048], replicated, may hold values from 0.1 to 1.9
- w_query: bfloat16 [2048, 1024], P(None, 'tp'), may hold values from -0.125 to 0.125
- w_key: bfloat16 [2048, 512], P(None, 'tp'), may hold values from -0.125 to 0.125
- w_value: bfloat16 [2048, 512], P(None, 'tp'), may hold values from -0.125 to 0.125
- query_gain: float32 [64], replicated, may hold values from 0.1 to 1.9
- key_gain: float32 [64], replicated, may hold values from 0.1 to 1.9
- sink_logit: float32 [16], P('tp'), may hold values from 4 to 8
- w_output: bfloat16 [1024, 2048], P('tp'), may hold values from -1.5 to 1.5
- x_experts: bfloat16 [3072, 2048], P('ep'), may hold values from -6 to 6
- expert_gain: float32 [2048], replicated, may hold values from 0.1 to 1.9
- routes: int32 [3072, 2], P('ep'), may hold values from 0 to 7, all different within a row; in each aligned block of 384 rows (0 to 383, 384 to 767, ...) at most 144 rows name the same one
- group_prob: float32 [3072], P('ep'), may hold values from 0.3 to 1
- expert_prob: float32 [3072, 2], P('ep'), may hold values from 0.05 to 1
- w_gate: bfloat16 [8, 2048, 1024], P('ep', None, 'tp'), may hold values from -0.125 to 0.125
- w_up: bfloat16 [8, 2048, 1024], P('ep', None, 'tp'), may hold values from -0.125 to 0.125
- w_down: bfloat16 [8, 1024, 2048], P('ep', 'tp'), may hold values from -0.1875 to 0.1875
Outputs:
- attend_out: bfloat16 [4096, 2048], P(('ep', 'tp'))
- expert_out: bfloat16 [3072, 2048], P('ep', 'tp')
Inputs may be any that keep to these rules, and one draw needn't show every extreme that they name: `routes`: each row names 2 different experts. Among the rows of one device no expert is named more than 144 times, and in every draw some expert is named exactly 144 times by one device's rows.
All inputs are finite; a program needn't handle non-finite values.
Results may differ from a plain program's by a relative error of at most 0.012.
Values may be sent and summed in bfloat16 or wider, within the bound.
A program may use at most 64 MiB of HBM per device.

v0:
```python
import jax
import jax.numpy as jnp
from jax import lax
from jax.sharding import PartitionSpec as P

HEAD_DIM = 64
WINDOW = 128
GRID_W = 64


epsilon = 1e-06
rope_base = 10000.0


def extended(x, sides, width):
    for axis, dim in sides:
        peers, length = (lax.axis_size(axis), x.shape[dim])
        up = [(i, (i + 1) % peers) for i in range(peers - 1)]
        down = [(j, i) for i, j in up]
        last = lax.slice_in_dim(x, length - width, length, axis=dim)
        initial = lax.slice_in_dim(x, 0, width, axis=dim)
        before = lax.ppermute(last, axis, up)
        after = lax.ppermute(initial, axis, down)
        x = jnp.concatenate([before, x, after], axis=dim)
    return x


def rms_scale(inputs, gain):
    values_f = inputs.astype(jnp.float32)
    scaled = values_f * lax.rsqrt(jnp.mean(values_f * values_f, axis=-1, keepdims=True) + epsilon)
    return (scaled * gain).astype(jnp.bfloat16)


def rope_tables(positions):
    grid_rows = (positions // GRID_W).astype(jnp.float32)
    grid_cols = (positions % GRID_W).astype(jnp.float32)
    half_dim = HEAD_DIM // 2
    inverse = rope_base ** (-jnp.arange(0, half_dim, 2, dtype=jnp.float32) / half_dim)
    angles = jnp.concatenate([grid_rows[:, None] * inverse, grid_cols[:, None] * inverse], axis=-1)
    return (jnp.cos(angles), jnp.sin(angles))


def head_norm_rope(projected, gain, cosine, sine_tab):
    scaled = (
        projected
        * lax.rsqrt(jnp.mean(projected * projected, axis=-1, keepdims=True) + epsilon)
        * gain
    )
    first_half, second_half = jnp.split(scaled, 2, axis=-1)
    cos_b = cosine[:, None, :]
    sin_b = sine_tab[:, None, :]
    turned = jnp.concatenate(
        [first_half * cos_b - second_half * sin_b, second_half * cos_b + first_half * sin_b],
        axis=-1,
    )
    return turned.astype(jnp.bfloat16)


def per_device(
    x_attend,
    attend_gain,
    w_query,
    w_key,
    w_value,
    query_gain,
    key_gain,
    sink_logit,
    w_output,
    x_experts,
    expert_gain,
    routes,
    group_prob,
    expert_prob,
    w_gate,
    w_up,
    w_down,
):
    tok_rows = x_attend.shape[0]
    model_width = x_attend.shape[1]
    heads_local = sink_logit.shape[0]
    kv_local = w_key.shape[1] // HEAD_DIM
    group = heads_local // kv_local
    offset = lax.axis_index("ep") * tok_rows
    positions = offset + jnp.arange(tok_rows, dtype=jnp.int32)
    cosine, sine_tab = rope_tables(positions)
    normed = rms_scale(x_attend, attend_gain)
    queries = head_norm_rope(
        jnp.dot(normed, w_query, preferred_element_type=jnp.float32).reshape(
            tok_rows, heads_local, HEAD_DIM
        ),
        query_gain,
        cosine,
        sine_tab,
    )
    key_rows = head_norm_rope(
        jnp.dot(normed, w_key, preferred_element_type=jnp.float32).reshape(
            tok_rows, kv_local, HEAD_DIM
        ),
        key_gain,
        cosine,
        sine_tab,
    )
    values = jnp.dot(normed, w_value, preferred_element_type=jnp.float32).astype(jnp.bfloat16)
    stacked = jnp.stack([key_rows.reshape(tok_rows, kv_local * HEAD_DIM), values], axis=0)
    padded = extended(stacked, (("ep", 1),), WINDOW)
    span_keys = padded[0].reshape(tok_rows + 2 * WINDOW, kv_local, HEAD_DIM)
    span_values = padded[1].reshape(tok_rows + 2 * WINDOW, kv_local, HEAD_DIM)
    scores = jnp.einsum(
        "qhgd,khd->hgqk",
        queries.reshape(tok_rows, kv_local, group, HEAD_DIM),
        span_keys,
        preferred_element_type=jnp.float32,
    ) * HEAD_DIM ** (-0.5)
    key_pos = offset - WINDOW + jnp.arange(tok_rows + 2 * WINDOW, dtype=jnp.int32)
    total_len = tok_rows * lax.axis_size("ep")
    in_window = (
        (jnp.abs(positions[:, None] - key_pos[None, :]) <= WINDOW)
        & (key_pos[None, :] >= 0)
        & (key_pos[None, :] < total_len)
    )
    scores = jnp.where(in_window[None, None], scores, -1e30)
    sink_col = sink_logit.reshape(kv_local, group)[:, :, None]
    peak = jnp.maximum(jnp.max(scores, axis=-1), sink_col)[..., None]
    weights = jnp.exp(scores - peak)
    denominator = jnp.sum(weights, axis=-1, keepdims=True) + jnp.exp(sink_col[..., None] - peak)
    probs = (weights / denominator).astype(jnp.bfloat16)
    attended = jnp.einsum("hgqk,khd->qhgd", probs, span_values, preferred_element_type=jnp.float32)
    attended = attended.astype(jnp.bfloat16).reshape(tok_rows, heads_local * HEAD_DIM)
    rows_in = attended
    attend_out = lax.psum_scatter(
        jnp.dot(rows_in, w_output, preferred_element_type=jnp.float32).astype(jnp.bfloat16),
        "tp",
        scatter_dimension=0,
        tiled=True,
    )
    moe_rows = x_experts.shape[0]
    top_count = routes.shape[1]
    experts_n = lax.axis_size("ep")
    tp_count = lax.axis_size("tp")
    capacity = max(2, (3 * moe_rows * top_count + 2 * experts_n - 1) // (2 * experts_n))
    moe_normed = rms_scale(x_experts, expert_gain)
    flat_ids = routes.reshape(-1)
    onehot = (flat_ids[:, None] == jnp.arange(experts_n, dtype=jnp.int32)[None, :]).astype(
        jnp.int32
    )
    rank_in = jnp.cumsum(onehot, axis=0) - onehot
    slot_pos = jnp.sum(rank_in * onehot, axis=1)
    dest_slot = flat_ids * capacity + slot_pos
    owner_tok = jnp.arange(moe_rows * top_count, dtype=jnp.int32) // top_count
    slot_tok = jnp.full((experts_n * capacity,), moe_rows, jnp.int32).at[dest_slot].set(owner_tok)
    gate_mat = w_gate[0]
    up_mat = w_up[0]
    down_mat = w_down[0]
    col_width = model_width // tp_count
    own_cols = lax.dynamic_slice_in_dim(moe_normed, lax.axis_index("tp") * col_width, col_width, 1)
    padded_rows = jnp.concatenate([own_cols, jnp.zeros((1, col_width), jnp.bfloat16)], axis=0)
    outgoing = padded_rows[slot_tok].reshape(experts_n, capacity, col_width)
    arrived = lax.all_to_all(outgoing, "ep", split_axis=0, concat_axis=0, tiled=True)
    col_piece = lax.all_gather(arrived, "tp", axis=2, tiled=True)
    rows_in = col_piece.reshape(experts_n * capacity, col_piece.shape[2])
    gate_act = jnp.dot(rows_in, gate_mat, preferred_element_type=jnp.float32)
    up_act = jnp.dot(rows_in, up_mat, preferred_element_type=jnp.float32)
    hidden = (jax.nn.silu(gate_act) * up_act).astype(jnp.bfloat16)
    partial_value = jnp.dot(hidden, down_mat, preferred_element_type=jnp.float32).astype(
        jnp.bfloat16
    )
    summed = (
        lax.psum_scatter(partial_value, "tp", scatter_dimension=1, tiled=True)
        .astype(jnp.float32)
        .astype(jnp.bfloat16)
    )
    summed = summed.reshape(experts_n, capacity, summed.shape[1])
    returned = lax.all_to_all(summed, "ep", split_axis=0, concat_axis=0, tiled=True)
    returned = returned.reshape(experts_n * capacity, returned.shape[2])
    picked = returned[dest_slot].astype(jnp.float32)
    route_weight = group_prob[:, None] * expert_prob / jnp.sum(expert_prob, axis=1, keepdims=True)
    expert_out = jnp.sum(
        picked.reshape(moe_rows, top_count, picked.shape[1]) * route_weight[:, :, None], axis=1
    )
    return (attend_out, expert_out.astype(jnp.bfloat16))


def solution(mesh):
    placed = (
        P("ep", None),
        P(),
        P(None, "tp"),
        P(None, "tp"),
        P(None, "tp"),
        P(),
        P(),
        P("tp"),
        P("tp", None),
        P("ep", None),
        P(),
        P("ep", None),
        P("ep"),
        P("ep", None),
        P("ep", None, "tp"),
        P("ep", None, "tp"),
        P("ep", "tp", None),
    )
    return jax.shard_map(
        per_device,
        mesh=mesh,
        in_specs=placed,
        out_specs=(P(("ep", "tp"), None), P("ep", "tp")),
        check_vma=False,
    )
```

profile of v0, /device:TPU:0, one launch (start us, length us, event | category | flops | bytes accessed | tf_op | source)
XLA Modules:
  0.0 207.4 jit_solution(12722982645366641306)
XLA Ops:
  7.2 3.6 %convert_element_type.89 = f32[384,2048]{1,0:T(8,128)} convert(bf16[384,2048]{1,0:T(8,128)(2,1)} %param.26) | non-fusion elementwise | flops 786432 | bytes 4718592 | tf_op jit(solution)/shard_map/convert_element_type | solution.py:29
  11.7 1.7 reduce-window.6
  14.3 3.4 %scatter_custom_fusion = s32[1152]{0:T(1024)S(1)} fusion(s32[768]{0:T(1024)S(1)} %fusion.40, s32[768]{0:T(1024)S(1)} %add_select_fusion, s32[]{:T(128)} %constant.107.clone.1), kind=kCustom, calls=%fused_computation.78 | custom fusion | bytes 4612 | tf_op jit(solution)/shard_map/scatter | solution.py:150
  17.7 0.8 dynamic-slice
  18.5 1.3 fusion.22
  19.8 4.2 %gather_fusion = bf16[1152,512]{1,0:T(8,128)(2,1)S(1)} fusion(bf16[385,512]{1,0:T(8,128)(2,1)S(1)} %concatenate.36, s32[2048]{0:T(1024)S(1)} %pad_clamp_fusion), kind=kCustom, calls=%fused_computation | custom fusion | bytes 2363904 | tf_op jit(solution)/shard_map/gather | solution.py:157
  24.1 36.2 %all_to_all.10 = bf16[8,144,512]{2,1,0:T(8,128)(2,1)} all-to-all(bf16[8,144,512]{2,1,0:T(8,128)(2,1)S(1)} %bitcast.69), channel_id=1, replica_groups=mesh['ep'=8,'tp'=4] {'ep'}, dimensions={0} | all-to-all | bytes 2359296 | tf_op jit(solution)/shard_map/all_to_all | solution.py:158
  60.4 36.2 %all-gather.2.cloned.1.call-done = bf16[8,144,2048]{2,1,0:T(8,128)(2,1)} async-done(((bf16[8,144,512]{2,1,0:T(8,128)(2,1)}), bf16[8,144,2048]{2,1,0:T(8,128)(2,1)}) %all-gather.2.cloned.1.call-update) | async-done | bytes 4718608 | tf_op jit(solution)/shard_map/all_gather | solution.py:159
  96.6 4.8 %fusion.19 = f32[1152,256]{1,0:T(8,128)} fusion(bf16[1152,2048]{1,0:T(8,128)(2,1)} %bitcast.79, bf16[1,2048,256]{2,1,0:T(8,128)(2,1)S(1)} %copy-done.9), kind=kOutput, calls=%fused_computation.33 | convolution fusion | flops 1207959552 | bytes 6946816 | tf_op jit(solution)/shard_map/dot_general | solution.py:161
  101.4 9.7 %convolution_convert_fusion = bf16[1152,2048]{1,0:T(8,128)(2,1)} fusion(bf16[1152,2048]{1,0:T(8,128)(2,1)} %bitcast.80, f32[1152,256]{1,0:T(8,128)} %fusion.19, bf16[1,256,2048]{2,1,0:T(8,128)(2,1)S(1)} %copy-done, bf16[1,2048,256]{2,1,0:T(8,128)(2,1)S(1)} %copy-done.10), kind=kOutput, calls=%fused_computation.3 | convolution fusion | flops 2420047872 | bytes 12713984 | tf_op jit(solution)/shard_map/dot_general | solution.py:164
  111.6 1.2 copy-done.2
  112.7 0.5 fusion.2
  113.2 2.0 multiply_reduce_fusion.3
  115.5 1.9 fusion.15
  117.4 0.7 pad_maximum_fusion.3
  118.1 3.9 %collective-permute-start = (bf16[2,128,128]{2,1,0:T(8,128)(2,1)}, bf16[2,128,128]{2,1,0:T(8,128)(2,1)}, u32[]{:S(2)}, u32[]{:S(2)}) collective-permute-start(bf16[2,128,128]{2,1,0:T(8,128)(2,1)} %get-tuple-element.8), channel_id=1, source_target_pairs={{0,4},{4,8},{8,12},{12,16},{16,20},{20,24},{24,28},{1,5},{5,9},{9,... | collective-permute-start | bytes 196616 | tf_op jit(solution)/shard_map/ppermute | solution.py:22
  122.0 1.5 collective-permute-start.1
  123.6 2.2 %multiply_reduce_fusion.2 = (f32[512,4]{0,1:T(4,128)S(1)}, f32[512,256]{0,1:T(8,128)S(1)}) fusion(bf16[2048,256]{1,0:T(8,128)(2,1)} %param.19, bf16[512,2048]{1,0:T(8,128)(2,1)S(1)} %copy-done.2, f32[2048]{0:T(1024)} %param.18, f32[512]{0:T(512)S(1)} %add_rsqrt_fusion.3), kind=kOutput, calls=%fused_computation.40 | convolution fusion | flops 541325312 | bytes 3688448 | tf_op jit(solution)/shard_map/dot_general | solution.py:88
  126.0 0.8 fusion.8
  126.9 1.6 collective-permute-done.1
  128.5 0.9 pad_maximum_fusion
  129.7 1.3 fusion.1
  131.1 1.4 fusion
  132.6 1.9 fusion.9
  134.5 2.1 %convolution_convert_fusion.1 = bf16[512,2048]{1,0:T(8,128)(2,1)} fusion(bf16[512,256]{0,1:T(8,128)(2,1)S(1)} %bitcast.71, bf16[256,2048]{1,0:T(8,128)(2,1)S(1)} %copy-done.3), kind=kOutput, calls=%fused_computation.16 | convolution fusion | flops 537919488 | bytes 3407872 | tf_op jit(solution)/shard_map/dot_general | solution.py:131
  136.7 22.5 %reduce-scatter.5.cloned.1.call-done = bf16[1152,512]{1,0:T(8,128)(2,1)} async-done(((bf16[1152,2048]{1,0:T(8,128)(2,1)}), bf16[1152,512]{1,0:T(8,128)(2,1)}) %reduce-scatter.5.cloned.1.call-update) | async-done | bytes 1179664 | tf_op jit(solution)/shard_map/reduce_scatter | solution.py:168
  159.2 5.5 %all-to-all-start.1 = ((bf16[8,144,512]{2,1,0:T(8,128)(2,1)}), bf16[8,144,512]{2,1,0:T(8,128)(2,1)S(1)}, u32[]{:S(2)}, u32[]{:S(2)}) async-start(bf16[8,144,512]{2,1,0:T(8,128)(2,1)} %bitcast.70), calls=%async_computation.3 | async-start | bytes 2359296 | tf_op jit(solution)/shard_map/all_to_all | solution.py:173
  164.7 0.8 copy.35
  165.5 27.5 %all-to-all-done.1 = bf16[8,144,512]{2,1,0:T(8,128)(2,1)S(1)} async-done(((bf16[8,144,512]{2,1,0:T(8,128)(2,1)}), bf16[8,144,512]{2,1,0:T(8,128)(2,1)S(1)}, u32[]{:S(2)}, u32[]{:S(2)}) %all-to-all-start.1) | async-done | bytes 1179680 | tf_op jit(solution)/shard_map/all_to_all | solution.py:173
  193.1 2.7 %gather_fusion.1 = bf16[768,512]{1,0:T(8,128)(2,1)S(1)} fusion(bf16[1152,512]{1,0:T(8,128)(2,1)S(1)} %bitcast.68, s32[1024]{0:T(1024)S(1)} %pad_clamp_fusion.1), kind=kCustom, calls=%fused_computation.1 | custom fusion | bytes 1575936 | tf_op jit(solution)/shard_map/gather | solution.py:175
  195.7 1.0 reshape.323
  196.7 4.1 %multiply_reduce_fusion.1 = bf16[384,512]{1,0:T(8,128)(2,1)} fusion(f32[384,2,512]{2,1,0:T(2,128)S(1)} %reshape.323, f32[384,2]{1,0:T(8,128)} %copy.35), kind=kLoop, calls=%fused_computation.19 | loop fusion | flops 589824 | bytes 1969152 | tf_op jit(solution)/shard_map/reduce_sum | solution.py:177
  (77 shorter events, 3.4 us)
Async XLA Ops:
  7.2 94.3 %copy-start = (bf16[1,256,2048]{2,1,0:T(8,128)(2,1)S(1)}, bf16[1,256,2048]{2,1,0:T(8,128)(2,1)}, u32[]{:S(2)}) copy-start(bf16[1,256,2048]{2,1,0:T(8,128)(2,1)} %param.33) | copy-start | bytes 3145732
  7.2 3.7 %copy-start.1 = (bf16[384,2048]{1,0:T(8,128)(2,1)S(1)}, bf16[384,2048]{1,0:T(8,128)(2,1)}, u32[]{:S(2)}) copy-start(bf16[384,2048]{1,0:T(8,128)(2,1)} %param.26) | copy-start | bytes 4718596
  7.2 89.4 %all-gather.2.cloned.1.call-start = ((), (), s32[]{:S(2)}) async-start(), calls=%async_computation.5 | async-start | bytes 5898240 | tf_op jit(solution)/shard_map/all_gather | solution.py:159
  7.2 4.0 %copy-start.5 = (s32[384,2]{0,1:T(2,128)S(1)}, s32[384,2]{0,1:T(2,128)}, u32[]{:S(2)}) copy-start(s32[384,2]{0,1:T(2,128)} %param.28) | copy-start | bytes 9220
  24.1 72.6 %copy-start.9 = (bf16[1,2048,256]{2,1,0:T(8,128)(2,1)S(1)}, bf16[1,2048,256]{2,1,0:T(8,128)(2,1)}, u32[]{:S(2)}) copy-start(bf16[1,2048,256]{2,1,0:T(8,128)(2,1)} %param.31) | copy-start | bytes 3145732
  60.3 98.8 %reduce-scatter.5.cloned.1.call-start = ((), (), s32[]{:S(2)}) async-start(), calls=%async_computation.6 | async-start | bytes 5898240 | tf_op jit(solution)/shard_map/reduce_scatter | solution.py:168
  96.6 4.8 %copy-start.10 = (bf16[1,2048,256]{2,1,0:T(8,128)(2,1)S(1)}, bf16[1,2048,256]{2,1,0:T(8,128)(2,1)}, u32[]{:S(2)}) copy-start(bf16[1,2048,256]{2,1,0:T(8,128)(2,1)} %param.32) | copy-start | bytes 3145732
  111.1 1.6 copy-start.2
  111.1 2.1 %copy-start.11 = (f32[2048]{0:T(1024)S(1)}, f32[2048]{0:T(1024)}, u32[]{:S(2)}) copy-start(f32[2048]{0:T(1024)} %param.18) | copy-start | bytes 24580
  111.2 89.7 %reduce-scatter.3.cloned.1.call-start = ((), (), s32[]{:S(2)}) async-start(), calls=%async_computation.4 | async-start | bytes 2621440 | tf_op jit(solution)/shard_map/reduce_scatter | solution.py:130
  112.7 2.5 %copy-start.7 = (f32[64]{0:T(128)S(1)}, f32[64]{0:T(128)}, u32[]{:S(2)}) copy-start(f32[64]{0:T(128)} %param.23) | copy-start | bytes 772
  117.4 8.4 %copy-start.8 = (f32[64]{0:T(128)S(1)}, f32[64]{0:T(128)}, u32[]{:S(2)}) copy-start(f32[64]{0:T(128)} %param.22) | copy-start | bytes 772
  118.1 8.8 %collective-permute-start = (bf16[2,128,128]{2,1,0:T(8,128)(2,1)}, bf16[2,128,128]{2,1,0:T(8,128)(2,1)}, u32[]{:S(2)}, u32[]{:S(2)}) collective-permute-start(bf16[2,128,128]{2,1,0:T(8,128)(2,1)} %get-tuple-element.8), channel_id=1, source_target_pairs={{0,4},{4,8},{8,12},{12,16},{16,20},{20,24},{24,28},{1,5},{5,9},{9,... | collective-permute-start | bytes 196616 | tf_op jit(solution)/shard_map/ppermute | solution.py:22
  122.0 6.5 %collective-permute-start.1 = (bf16[2,128,128]{2,1,0:T(8,128)(2,1)}, bf16[2,128,128]{2,1,0:T(8,128)(2,1)}, u32[]{:S(2)}, u32[]{:S(2)}) collective-permute-start(bf16[2,128,128]{2,1,0:T(8,128)(2,1)} %get-tuple-element.9), channel_id=1, source_target_pairs={{4,0},{8,4},{12,8},{16,12},{20,16},{24,20},{28,24},{5,1},{9,5},{13... | collective-permute-start | bytes 196616 | tf_op jit(solution)/shard_map/ppermute | solution.py:23
  123.5 3.2 %copy-start.12 = (f32[4]{0:T(128)S(1)}, f32[4]{0:T(128)}, u32[]{:S(2)}) copy-start(f32[4]{0:T(128)} %param.24) | copy-start | bytes 52
  132.6 2.0 copy-start.3
  136.6 28.0 %copy-start.4 = (f32[384,2]{0,1:T(2,128)S(1)}, f32[384,2]{0,1:T(2,128)}, u32[]{:S(2)}) copy-start(f32[384,2]{0,1:T(2,128)} %param.30) | copy-start | bytes 9220
  136.6 28.1 %copy-start.6 = (f32[384]{0:T(512)S(1)}, f32[384]{0:T(512)}, u32[]{:S(2)}) copy-start(f32[384]{0:T(512)} %param.29) | copy-start | bytes 4612
  159.2 33.9 %all-to-all-start.1 = ((bf16[8,144,512]{2,1,0:T(8,128)(2,1)}), bf16[8,144,512]{2,1,0:T(8,128)(2,1)S(1)}, u32[]{:S(2)}, u32[]{:S(2)}) async-start(bf16[8,144,512]{2,1,0:T(8,128)(2,1)} %bitcast.70), calls=%async_computation.3 | async-start | bytes 2359296 | tf_op jit(solution)/shard_map/all_to_all | solution.py:173
Sparse Core Ops, SparseCore 0:
  60.4 36.1 all-gather.1
  111.3 47.8 reduce-scatter.4
  162.3 31.1 reduce-scatter.2
where the time goes:
time: 208 us; the launch traced here: 207 us
  waiting for transfers between devices  88 us (42%)
  blocking collectives  36.2 us (17%)
  matrix products  25.9 us (12%)
  other arithmetic  16.5 us (8%)
  local copies, waits for them, and re-layouts  15.6 us (8%)
  between operations  14.2 us (7%)
  starting transfers between devices  11 us (5%)
    all_gather x1, waiting for transfers between devices, per_device(): col_piece = lax.all_gather(arrived, 'tp', axis=2, tiled=True)  36.2 us
    all_to_all x1, blocking collectives, per_device(): lax.all_to_all(outgoing, 'ep', split_axis=0, concat_axis=0, tiled=True)  36.2 us
    all_to_all x1, waiting for transfers between devices, per_device(): lax.all_to_all(summed, 'ep', split_axis=0, concat_axis=0, tiled=True)  27.5 us
    reduce_scatter x1, waiting for transfers between devices, per_device(): lax.psum_scatter(partial_value, 'tp', scatter_dimension=1, tiled=True)  22.5 us
    dot_general x1, matrix products, per_device(): jnp.dot(hidden, down_mat, preferred_element_type=jnp.float32)  9.69 us
    all_to_all x1, starting transfers between devices, per_device(): lax.all_to_all(summed, 'ep', split_axis=0, concat_axis=0, tiled=True)  5.52 us
    dot_general x1, matrix products, per_device(): gate_act = jnp.dot(rows_in, gate_mat, preferred_element_type=jnp.float32)  4.82 us
    gather x1, local copies, waits for them, and re-layouts, per_device(): outgoing = padded_rows[slot_tok].reshape(experts_n, capacity, col_width)  4.24 us
  transfers between devices with their start and end apart: 6, of which 4 were waited for; matrix products, arithmetic and copies ran while one was open for 12% of the time, Pallas kernels for 0%

commit v1 on v0

--- a/solution.py
+++ b/solution.py
@@ -1,11 +1,16 @@
+import functools
+
 import jax
 import jax.numpy as jnp
 from jax import lax
+from jax.experimental import pallas as pl
+from jax.experimental.pallas import tpu as pltpu
 from jax.sharding import PartitionSpec as P
 
 HEAD_DIM = 64
 WINDOW = 128
 GRID_W = 64
+MESH = pl.DeviceIdType.MESH
 
 
 epsilon = 1e-06
@@ -54,6 +59,242 @@
         axis=-1,
     )
     return turned.astype(jnp.bfloat16)
+
+
+def flip(a, b, count):
+    total, bit = 0, 1
+    while bit < count:
+        total = total + lax.rem(a // bit + b // bit, 2) * bit
+        bit *= 2
+    return total
+
+
+def exchange_kernel(
+    n_ep,
+    send_ref,
+    gate_ref,
+    up_ref,
+    down_ref,
+    mix_ref,
+    attn_ref,
+    out_ref,
+    attn_out_ref,
+    rows_buf,
+    part_out,
+    part_keep,
+    part_in,
+    y_out,
+    y_own,
+    y_in,
+    final,
+    back,
+    total,
+    attn_in,
+    attn_y_out,
+    attn_y_in,
+    local_sem,
+    d_send, d_recv,
+    p_send, p_recv,
+    y_send, y_recv,
+    r_send, r_recv,
+    c_send, c_recv,
+    s_send, s_recv,
+    f_send, f_recv,
+    a_send, a_recv,
+):
+    me = lax.axis_index("ep")
+    lane = lax.axis_index("tp")
+    core = lax.rem(lane, 2)
+    side = lane // 2
+    other_core, other_side = 1 - core, 1 - side
+    partner = 2 * side + other_core
+    across = 2 * other_side + core
+    width = send_ref.shape[2]
+
+    barrier = pltpu.get_barrier_semaphore()
+
+    def greet(k, carry):
+        pl.semaphore_signal(
+            barrier, inc=1, device_id={"ep": flip(me, k, n_ep), "tp": lane}, device_id_type=MESH
+        )
+        return carry
+
+    lax.fori_loop(1, n_ep, greet, 0)
+    for peer in (partner, across):
+        pl.semaphore_signal(barrier, inc=1, device_id={"ep": me, "tp": peer}, device_id_type=MESH)
+    pl.semaphore_wait(barrier, n_ep + 1)
+
+    def remote(src, dst, sends, recvs, k, ep, tp):
+        return pltpu.make_async_remote_copy(
+            src_ref=src,
+            dst_ref=dst,
+            send_sem=sends.at[k],
+            recv_sem=recvs.at[k],
+            device_id={"ep": ep, "tp": tp},
+            device_id_type=MESH,
+        )
+
+    def dispatch(k):
+        dest = flip(me, k, n_ep)
+        return remote(send_ref.at[dest], rows_buf.at[lane, k], d_send, d_recv, k, dest, lane)
+
+    def to_partner(k):
+        block = rows_buf.at[lane, k]
+        return remote(block, block, p_send, p_recv, k, me, partner)
+
+    def to_across(k):
+        block = rows_buf.at[lane, k]
+        return remote(block, block, y_send, y_recv, k, me, across)
+
+    def relay(k):
+        block = rows_buf.at[across, k]
+        return remote(block, block, r_send, r_recv, k, me, partner)
+
+    def sum_core(k):
+        return remote(part_out.at[k], part_in.at[k], c_send, c_recv, k, me, partner)
+
+    def sum_side(k):
+        return remote(y_out.at[k], y_in.at[k], s_send, s_recv, k, me, across)
+
+    def give_back(k):
+        return remote(final.at[k], back.at[k], f_send, f_recv, k, flip(me, k, n_ep), lane)
+
+    def attn_core(s):
+        return remote(
+            attn_ref.at[2 * s + other_core], attn_in.at[s], a_send, a_recv, s, me, partner
+        )
+
+    def attn_side():
+        return remote(attn_y_out, attn_y_in, a_send, a_recv, 2, me, across)
+
+    own = pltpu.make_async_copy(send_ref.at[me], rows_buf.at[lane, 0], local_sem)
+    own.start()
+
+    def start_dispatch(k, carry):
+        dispatch(k).start()
+        return carry
+
+    lax.fori_loop(1, n_ep, start_dispatch, 0)
+    attn_core(0).start()
+    attn_core(1).start()
+    total[...] = jnp.zeros_like(total)
+    own.wait()
+
+    def step(t, carry):
+        @pl.when(t < n_ep)
+        def _():
+            @pl.when(t > 0)
+            def _():
+                dispatch(t).wait_recv()
+
+            to_partner(t).start()
+            to_across(t).start()
+
+        k5 = t - 3
+
+        @pl.when((k5 >= 0) & (k5 < n_ep))
+        def _():
+            sum_core(k5).wait_recv()
+            y_out[k5] = (
+                part_keep[k5, other_side].astype(jnp.float32)
+                + part_in[k5, other_side].astype(jnp.float32)
+            ).astype(jnp.bfloat16)
+            sum_side(k5).start()
+            y_own[k5] = part_keep[k5, side].astype(jnp.float32) + part_in[k5, side].astype(
+                jnp.float32
+            )
+
+        k1 = t - 1
+
+        @pl.when((k1 >= 0) & (k1 < n_ep))
+        def _():
+            to_across(k1).wait_recv()
+            relay(k1).start()
+
+        k2 = t - 2
+
+        @pl.when((k2 >= 0) & (k2 < n_ep))
+        def _():
+            to_partner(k2).wait_recv()
+            relay(k2).wait_recv()
+            gate = jnp.zeros((send_ref.shape[1], gate_ref.shape[1]), jnp.float32)
+            up = gate
+            for q in range(4):
+                rows = rows_buf[q, k2]
+                span = slice(q * width, (q + 1) * width)
+                gate += jnp.dot(rows, gate_ref[span, :], preferred_element_type=jnp.float32)
+                up += jnp.dot(rows, up_ref[span, :], preferred_element_type=jnp.float32)
+            hidden = (gate / (1.0 + jnp.exp(-gate)) * up).astype(jnp.bfloat16)
+            for s in range(2):
+                for c, target in ((other_core, part_out), (core, part_keep)):
+                    start = pl.multiple_of((2 * s + c) * width, width)
+                    target[k2, s] = jnp.dot(
+                        hidden, down_ref[:, pl.ds(start, width)], preferred_element_type=jnp.float32
+                    ).astype(jnp.bfloat16)
+            sum_core(k2).start()
+
+        k6 = t - 4
+
+        @pl.when((k6 >= 0) & (k6 < n_ep))
+        def _():
+            sum_side(k6).wait_recv()
+            final[k6] = (y_own[k6] + y_in[k6].astype(jnp.float32)).astype(jnp.bfloat16)
+
+            @pl.when(k6 > 0)
+            def _():
+                give_back(k6).start()
+
+            @pl.when(k6 == 0)
+            def _():
+                total[...] += jnp.dot(mix_ref[me], final[0], preferred_element_type=jnp.float32)
+
+        k7 = t - 6
+
+        @pl.when((k7 > 0) & (k7 < n_ep))
+        def _():
+            give_back(k7).wait_recv()
+            total[...] += jnp.dot(
+                mix_ref[flip(me, k7, n_ep)], back[k7], preferred_element_type=jnp.float32
+            )
+
+        @pl.when(t == 1)
+        def _():
+            attn_core(0).wait_recv()
+            attn_core(1).wait_recv()
+            attn_y_out[...] = (
+                attn_ref[2 * other_side + core].astype(jnp.float32)
+                + attn_in[other_side].astype(jnp.float32)
+            ).astype(jnp.bfloat16)
+            attn_side().start()
+
+        return carry
+
+    lax.fori_loop(0, n_ep + 6, step, 0)
+    attn_side().wait_recv()
+    attn_out_ref[...] = (
+        attn_ref[2 * side + core].astype(jnp.float32)
+        + attn_in[side].astype(jnp.float32)
+        + attn_y_in[...].astype(jnp.float32)
+    ).astype(jnp.bfloat16)
+    out_ref[...] = total[...].astype(jnp.bfloat16)
+
+    def drain(k, carry):
+        @pl.when(k > 0)
+        def _():
+            dispatch(k).wait_send()
+            give_back(k).wait_send()
+
+        to_partner(k).wait_send()
+        to_across(k).wait_send()
+        relay(k).wait_send()
+        sum_core(k).wait_send()
+        sum_side(k).wait_send()
+        return carry
+
+    lax.fori_loop(0, n_ep, drain, 0)
+    attn_core(0).wait_send()
+    attn_core(1).wait_send()
+    attn_side().wait_send()
 
 
 def per_device(
@@ -126,58 +367,73 @@
     probs = (weights / denominator).astype(jnp.bfloat16)
     attended = jnp.einsum("hgqk,khd->qhgd", probs, span_values, preferred_element_type=jnp.float32)
     attended = attended.astype(jnp.bfloat16).reshape(tok_rows, heads_local * HEAD_DIM)
-    rows_in = attended
-    attend_out = lax.psum_scatter(
-        jnp.dot(rows_in, w_output, preferred_element_type=jnp.float32).astype(jnp.bfloat16),
-        "tp",
-        scatter_dimension=0,
-        tiled=True,
+    tp_count = lax.axis_size("tp")
+    attn_part = (
+        jnp.dot(attended, w_output, preferred_element_type=jnp.float32)
+        .astype(jnp.bfloat16)
+        .reshape(tp_count, tok_rows // tp_count, model_width)
     )
     moe_rows = x_experts.shape[0]
     top_count = routes.shape[1]
-    experts_n = lax.axis_size("ep")
-    tp_count = lax.axis_size("tp")
-    capacity = max(2, (3 * moe_rows * top_count + 2 * experts_n - 1) // (2 * experts_n))
+    n_ep = lax.axis_size("ep")
+    capacity = max(2, (3 * moe_rows * top_count + 2 * n_ep - 1) // (2 * n_ep))
     moe_normed = rms_scale(x_experts, expert_gain)
-    flat_ids = routes.reshape(-1)
-    onehot = (flat_ids[:, None] == jnp.arange(experts_n, dtype=jnp.int32)[None, :]).astype(
-        jnp.int32
-    )
-    rank_in = jnp.cumsum(onehot, axis=0) - onehot
-    slot_pos = jnp.sum(rank_in * onehot, axis=1)
-    dest_slot = flat_ids * capacity + slot_pos
-    owner_tok = jnp.arange(moe_rows * top_count, dtype=jnp.int32) // top_count
-    slot_tok = jnp.full((experts_n * capacity,), moe_rows, jnp.int32).at[dest_slot].set(owner_tok)
-    gate_mat = w_gate[0]
-    up_mat = w_up[0]
-    down_mat = w_down[0]
     col_width = model_width // tp_count
     own_cols = lax.dynamic_slice_in_dim(moe_normed, lax.axis_index("tp") * col_width, col_width, 1)
-    padded_rows = jnp.concatenate([own_cols, jnp.zeros((1, col_width), jnp.bfloat16)], axis=0)
-    outgoing = padded_rows[slot_tok].reshape(experts_n, capacity, col_width)
-    arrived = lax.all_to_all(outgoing, "ep", split_axis=0, concat_axis=0, tiled=True)
-    col_piece = lax.all_gather(arrived, "tp", axis=2, tiled=True)
-    rows_in = col_piece.reshape(experts_n * capacity, col_piece.shape[2])
-    gate_act = jnp.dot(rows_in, gate_mat, preferred_element_type=jnp.float32)
-    up_act = jnp.dot(rows_in, up_mat, preferred_element_type=jnp.float32)
-    hidden = (jax.nn.silu(gate_act) * up_act).astype(jnp.bfloat16)
-    partial_value = jnp.dot(hidden, down_mat, preferred_element_type=jnp.float32).astype(
-        jnp.bfloat16
-    )
-    summed = (
-        lax.psum_scatter(partial_value, "tp", scatter_dimension=1, tiled=True)
-        .astype(jnp.float32)
-        .astype(jnp.bfloat16)
-    )
-    summed = summed.reshape(experts_n, capacity, summed.shape[1])
-    returned = lax.all_to_all(summed, "ep", split_axis=0, concat_axis=0, tiled=True)
-    returned = returned.reshape(experts_n * capacity, returned.shape[2])
-    picked = returned[dest_slot].astype(jnp.float32)
     route_weight = group_prob[:, None] * expert_prob / jnp.sum(expert_prob, axis=1, keepdims=True)
-    expert_out = jnp.sum(
-        picked.reshape(moe_rows, top_count, picked.shape[1]) * route_weight[:, :, None], axis=1
-    )
-    return (attend_out, expert_out.astype(jnp.bfloat16))
+    names = jnp.arange(n_ep, dtype=jnp.int32)
+    chosen = routes[:, :, None] == names[None, None, :]
+    named = jnp.any(chosen, axis=1)
+    token = jnp.arange(moe_rows, dtype=jnp.int32)
+    earlier = (token[None, :] < token[:, None]).astype(jnp.bfloat16)
+    rank = jnp.dot(earlier, named.astype(jnp.bfloat16), preferred_element_type=jnp.float32)
+    rank = jnp.where(named, rank.astype(jnp.int32), -1)
+    share = jnp.sum(jnp.where(chosen, route_weight[:, :, None], 0.0), axis=1)
+    slots = jnp.arange(capacity, dtype=jnp.int32)
+    pick = (rank.T[:, None, :] == slots[None, :, None]).astype(jnp.bfloat16)
+    outgoing = jnp.dot(
+        pick.reshape(n_ep * capacity, moe_rows), own_cols, preferred_element_type=jnp.float32
+    )
+    outgoing = outgoing.astype(jnp.bfloat16).reshape(n_ep, capacity, col_width)
+    mix = jnp.where(
+        rank.T[:, :, None] == slots[None, None, :], share.T[:, :, None], 0.0
+    ).astype(jnp.bfloat16)
+    hidden_cols = w_gate.shape[2]
+    slice_rows = tok_rows // tp_count
+    bf16, f32 = jnp.bfloat16, jnp.float32
+    vmem = pl.BlockSpec(memory_space=pltpu.VMEM)
+    dma = pltpu.SemaphoreType.DMA
+    expert_out, attend_out = pl.pallas_call(
+        functools.partial(exchange_kernel, n_ep),
+        out_shape=(
+            jax.ShapeDtypeStruct((moe_rows, col_width), bf16),
+            jax.ShapeDtypeStruct((slice_rows, model_width), bf16),
+        ),
+        in_specs=[vmem] * 6,
+        out_specs=(vmem, vmem),
+        scratch_shapes=[
+            pltpu.VMEM((tp_count, n_ep, capacity, col_width), bf16),
+            pltpu.VMEM((n_ep, 2, capacity, col_width), bf16),
+            pltpu.VMEM((n_ep, 2, capacity, col_width), bf16),
+            pltpu.VMEM((n_ep, 2, capacity, col_width), bf16),
+            pltpu.VMEM((n_ep, capacity, col_width), bf16),
+            pltpu.VMEM((n_ep, capacity, col_width), f32),
+            pltpu.VMEM((n_ep, capacity, col_width), bf16),
+            pltpu.VMEM((n_ep, capacity, col_width), bf16),
+            pltpu.VMEM((n_ep, capacity, col_width), bf16),
+            pltpu.VMEM((moe_rows, col_width), f32),
+            pltpu.VMEM((2, slice_rows, model_width), bf16),
+            pltpu.VMEM((slice_rows, model_width), bf16),
+            pltpu.VMEM((slice_rows, model_width), bf16),
+            dma(()),
+        ]
+        + [dma((n_ep,))] * 14
+        + [dma((3,))] * 2,
+        compiler_params=pltpu.CompilerParams(
+            collective_id=0, has_side_effects=True, vmem_limit_bytes=60 * 1024 * 1024
+        ),
+    )(outgoing, w_gate[0], w_up[0], w_down[0], mix, attn_part)
+    return (attend_out, expert_out)
 
 
 def solution(mesh):

time: 208 us -> 132 us (0.63)
  Pallas kernels: 0 us -> 88.5 us
  waiting for transfers between devices: 88 us -> 0.01 us
  blocking collectives: 36.2 us -> 0 us
  between operations: 14.2 us -> 1.01 us
  local copies, waits for them, and re-layouts: 15.6 us -> 6.86 us
  matrix products: 25.9 us -> 17.5 us
  other arithmetic: 16.5 us -> 10.2 us
  starting transfers between devices: 11 us -> 6.34 us
    pallas_call x0 -> x1, Pallas kernels: none -> 88.5 us  [per_device(): pl.pallas_call(functools.partial(exchange_kernel, n_ep), out_shape=(jax.S...]
    all_gather x1 -> x0, waiting for transfers between devices: 36.2 us -> none  [per_device(): col_piece = lax.all_gather(arrived, 'tp', axis=2, tiled=True)]
    all_to_all x1 -> x0, blocking collectives: 36.2 us -> none  [per_device(): lax.all_to_all(outgoing, 'ep', split_axis=0, concat_axis=0, tiled=True)]
    all_to_all x1 -> x0, waiting for transfers between devices: 27.5 us -> none  [per_device(): lax.all_to_all(summed, 'ep', split_axis=0, concat_axis=0, tiled=True)]
    reduce_scatter x2 -> x0, waiting for transfers between devices: 22.5 us -> none  [the longest x1 22.5 us: per_device(): lax.psum_scatter(partial_value, 'tp', scatter_dimension=1, tiled=True)]
    dot_general x3, matrix products: 16.6 us -> 5.36 us  [the longest x1 3.13 us: per_device(): jnp.dot(pick.reshape(n_ep * capacity, moe_rows), own_cols, preferred_elem...]
    gather x2 -> x0, local copies, waits for them, and re-layouts: 6.91 us -> none  [the longest x1 4.24 us: per_device(): outgoing = padded_rows[slot_tok].reshape(experts_n, capacity, col_width)]
    all_to_all x1 -> x0, starting transfers between devices: 5.52 us -> none  [per_device(): lax.all_to_all(summed, 'ep', split_axis=0, concat_axis=0, tiled=True)]
  transfers between devices with their start and end apart: 6 -> 2, of which waited for: 4 -> 0; matrix products, arithmetic and copies ran while one was open for 12% -> 9% of each run, Pallas kernels for 0% -> 0%
where the time goes in v1:
time: 132 us; the launch traced here: 130 us
  Pallas kernels  88.5 us (67%)
  matrix products  17.5 us (13%)
  other arithmetic  10.2 us (8%)
  local copies, waits for them, and re-layouts  6.86 us (5%)
  starting transfers between devices  6.34 us (5%)
    pallas_call x1, Pallas kernels, per_device(): pl.pallas_call(functools.partial(exchange_kernel, n_ep), out_shape=(jax.S...  88.5 us
    unnamed x26, local copies, waits for them, and re-layouts  5.45 us
    ppermute x1, starting transfers between devices, extended(): before = lax.ppermute(last, axis, up)  4.87 us
    dot_general x1, matrix products, per_device(): jnp.einsum('hgqk,khd->qhgd', probs, span_values, preferred_element_type=j...  4.7 us
    dot_general x1, matrix products, per_device(): jnp.dot(pick.reshape(n_ep * capacity, moe_rows), own_cols, preferred_elem...  3.13 us
  transfers between devices with their start and end apart: 2, of which 0 were waited for; matrix products, arithmetic and copies ran while one was open for 9% of the time, Pallas kernels for 0%

profile of v1, /device:TPU:0, one launch (start us, length us, event | category | flops | bytes accessed | tf_op | source)
XLA Modules:
  0.0 130.3 jit_solution(15961828635743734229)
XLA Ops:
  0.7 2.2 %fusion.2 = f32[512]{0:T(512)S(1)} fusion(bf16[512,2048]{1,0:T(8,128)(2,1)} %param.17), kind=kLoop, calls=%fused_computation.7 | loop fusion | flops 3145216 | bytes 2099200 | tf_op jit(solution)/shard_map/reduce_sum | solution.py:35
  2.9 2.6 %multiply_reduce_fusion.2 = (f32[512,2]{0,1:T(2,128)S(1)}, f32[512,128]{0,1:T(8,128)S(1)}) fusion(bf16[2048,128]{1,0:T(8,128)(2,1)} %param.20, bf16[512,2048]{1,0:T(8,128)(2,1)} %param.17, f32[2048]{0:T(1024)} %param.18, f32[512]{0:T(512)S(1)} %add_rsqrt_fusion.2), kind=kOutput, calls=%fused_computation.41 | convolution fusion | flops 272759808 | bytes 2897920 | tf_op jit(solution)/shard_map/dot_general | solution.py:337
  5.6 0.2 fusion.21
  5.8 0.1 multiply_multiply_fusion.1
  6.0 0.1 copy.31
  6.1 2.6 %fusion.9 = bf16[1,512,128]{2,1,0:T(8,128)(2,1)S(1)} fusion(bf16[2048,128]{1,0:T(8,128)(2,1)} %param.21, bf16[512,2048]{1,0:T(8,128)(2,1)} %param.17, f32[2048]{0:T(1024)S(1)} %copy-done.10, f32[512]{0:T(512)S(1)} %add_rsqrt_fusion.2), kind=kOutput, calls=%fused_computation.22 | convolution fusion | flops 272695296 | bytes 2762752 | tf_op jit(solution)/shard_map/dot_general | solution.py:344
  8.7 4.9 %collective-permute-start = (bf16[2,128,128]{2,1,0:T(8,128)(2,1)S(1)}, bf16[2,128,128]{2,1,0:T(8,128)(2,1)S(1)}, u32[]{:S(2)}, u32[]{:S(2)}) collective-permute-start(bf16[2,128,128]{2,1,0:T(8,128)(2,1)S(1)} %get-tuple-element.12), channel_id=1, source_target_pairs={{0,4},{4,8},{8,12},{12,16},{16,20},{20,24},{24,28},{1,5},{5,9},{9,... | collective-permute-start | bytes 196616 | tf_op jit(solution)/shard_map/ppermute | solution.py:27
  13.6 1.5 %collective-permute-start.1 = (bf16[2,128,128]{2,1,0:T(8,128)(2,1)S(1)}, bf16[2,128,128]{2,1,0:T(8,128)(2,1)S(1)}, u32[]{:S(2)}, u32[]{:S(2)}) collective-permute-start(bf16[2,128,128]{2,1,0:T(8,128)(2,1)S(1)} %get-tuple-element.13), channel_id=1, source_target_pairs={{4,0},{8,4},{12,8},{16,12},{20,16},{24,20},{28,24},{5,1},{9,5},{13... | collective-permute-start | bytes 196616 | tf_op jit(solution)/shard_map/ppermute | solution.py:28
  15.1 2.0 %convert_element_type.68 = f32[384,2048]{1,0:T(8,128)} convert(bf16[384,2048]{1,0:T(8,128)(2,1)S(1)} %copy-done.2) | non-fusion elementwise | flops 786432 | bytes 4718592 | tf_op jit(solution)/shard_map/convert_element_type | solution.py:34
  17.2 0.4 multiply_reduce_fusion
  17.6 0.5 copy-done.9
  18.1 1.0 multiply_reduce_fusion.1
  19.1 0.1 multiply_multiply_fusion
  19.2 0.1 subtract_convert_fusion
  19.4 0.1 fusion.10
  19.7 0.3 bitcast_compare_fusion
  20.0 2.3 %select_convert_fusion.mix_ref = bf16[8,384,144]{2,1,0:T(8,128)(2,1)} fusion(bf16[8,384]{1,0:T(8,128)(2,1)S(1)} %bitcast.65, s32[8,384]{1,0:T(8,128)S(1)} %fusion.10), kind=kLoop, calls=%fused_computation.10 | loop fusion | flops 884736 | bytes 903168 | tf_op jit(solution)/shard_map/convert_element_type | solution.py:400
  22.3 0.8 dynamic-slice
  23.1 3.1 %convolution_convert_fusion.1 = bf16[1152,512]{1,0:T(8,128)(2,1)} fusion(pred[1152,384]{1,0:T(32,128)(4,1)S(1)} %bitcast_compare_fusion, f32[384,2048]{1,0:T(8,128)} %convert_element_type.68, s32[]{:T(128)S(6)} %select_n.41, f32[512]{0:T(512)S(1)} %dynamic-slice, f32[384]{0:T(512)S(1)} %add_rsqrt_fusion.3), kind=kOutput, calls=%fused_computation.15 | convolution fusion | flops 454164480 | bytes 2412036 | tf_op jit(solution)/shard_map/dot_general | solution.py:394
  26.2 0.7 fusion.7
  27.0 0.1 max.17
  27.1 0.1 copy.33
  27.3 1.3 fusion.1
  28.6 1.4 %fusion = f32[2,2,512]{2,1,0:T(2,128)S(1)} fusion(f32[2,768,512,2]{2,1,3,0:T(8,128)S(1)} %get-tuple-element.23, f32[2,2,512]{2,1,0:T(2,128)S(1)} %broadcast_maximum_fusion, pred[512,768]{0,1:T(8,128)(4,1)S(1)} %fusion.7), kind=kLoop, calls=%fused_computation.3 | loop fusion | flops 6289408 | bytes 6701056 | tf_op jit(solution)/shard_map/reduce_sum | solution.py:366
  30.0 1.2 copy-done.1
  31.2 0.1 exponential_add_fusion
  31.3 0.1 copy.32
  31.4 4.7 %fusion.8 = bf16[2,64,2,512]{3,1,2,0:T(8,128)(2,1)S(1)} fusion(bf16[768,2,64,1]{0,2,3,1:T(8,128)(2,1)S(1)} %bitcast.62, f32[2,768,512,2]{2,1,3,0:T(8,128)} %copy-done.1, f32[2,2,512]{2,1,0:T(2,128)S(1)} %exponential_add_fusion, f32[2,2,512]{2,1,0:T(2,128)S(1)} %broadcast_maximum_fusion, pred[512,768]{0,1:T(8,128)(4,1)S(1)} %fusion.7), kind=kOutput, calls=%fused_computation.20 | convolution fusion | flops 209321984 | bytes 7159808 | tf_op jit(solution)/shard_map/hgqk,khd->qhgd/dot_general | solution.py:368
  36.1 2.1 %convolution_convert_fusion = bf16[512,2048]{1,0:T(8,128)(2,1)} fusion(bf16[512,256]{0,1:T(8,128)(2,1)S(1)} %bitcast.59, bf16[256,2048]{1,0:T(8,128)(2,1)S(1)} %copy-done), kind=kOutput, calls=%fused_computation.14 | convolution fusion | flops 537919488 | bytes 3407872 | tf_op jit(solution)/shard_map/dot_general | solution.py:372
  38.2 88.5 %shard_map.176 = (bf16[384,512]{1,0:T(8,128)(2,1)}, bf16[128,2048]{1,0:T(8,128)(2,1)}) custom-call(bf16[8,144,512]{2,1,0:T(8,128)(2,1)} %bitcast.55, bf16[2048,256]{1,0:T(8,128)(2,1)} %bitcast.56, bf16[2048,256]{1,0:T(8,128)(2,1)} %bitcast.57, bf16[256,2048]{1,0:T(8,128)(2,1)} %bitcast.58, bf16[8,384,144]{2,1,0:T(8,128)(2,1)} %select_convert_fusion.mix_ref, ...), custom_call_target="tpu_custom_call" | custom-call | tf_op jit(solution)/shard_map/pallas_call | solution.py:406
  126.7 1.9 %copy.42 = bf16[128,2048]{1,0:T(8,128)(2,1)} copy(bf16[128,2048]{1,0:T(8,128)(2,1)} %get-tuple-element.30) | data formatting | bytes 1048576
  128.6 1.8 %copy.43 = bf16[384,512]{1,0:T(8,128)(2,1)} copy(bf16[384,512]{1,0:T(8,128)(2,1)} %get-tuple-element.31) | data formatting | bytes 786432
  (46 shorter events, 0.6 us)
Async XLA Ops:
  0.6 35.5 %copy-start = (bf16[256,2048]{1,0:T(8,128)(2,1)S(1)}, bf16[256,2048]{1,0:T(8,128)(2,1)}, u32[]{:S(2)}) copy-start(bf16[256,2048]{1,0:T(8,128)(2,1)} %param.25) | copy-start | bytes 3145732
  0.7 5.1 %copy-start.7 = (f32[64]{0:T(128)S(1)}, f32[64]{0:T(128)}, u32[]{:S(2)}) copy-start(f32[64]{0:T(128)} %param.23) | copy-start | bytes 772
  2.9 3.3 %copy-start.10 = (f32[2048]{0:T(1024)S(1)}, f32[2048]{0:T(1024)}, u32[]{:S(2)}) copy-start(f32[2048]{0:T(1024)} %param.18) | copy-start | bytes 24580
  5.9 9.2 %copy-start.2 = (bf16[384,2048]{1,0:T(8,128)(2,1)S(1)}, bf16[384,2048]{1,0:T(8,128)(2,1)}, u32[]{:S(2)}) copy-start(bf16[384,2048]{1,0:T(8,128)(2,1)} %param.26) | copy-start | bytes 4718596
  8.7 18.3 %collective-permute-start = (bf16[2,128,128]{2,1,0:T(8,128)(2,1)S(1)}, bf16[2,128,128]{2,1,0:T(8,128)(2,1)S(1)}, u32[]{:S(2)}, u32[]{:S(2)}) collective-permute-start(bf16[2,128,128]{2,1,0:T(8,128)(2,1)S(1)} %get-tuple-element.12), channel_id=1, source_target_pairs={{0,4},{4,8},{8,12},{12,16},{16,20},{20,24},{24,28},{1,5},{5,9},{9,... | collective-permute-start | bytes 196616 | tf_op jit(solution)/shard_map/ppermute | solution.py:27
  13.6 13.5 %collective-permute-start.1 = (bf16[2,128,128]{2,1,0:T(8,128)(2,1)S(1)}, bf16[2,128,128]{2,1,0:T(8,128)(2,1)S(1)}, u32[]{:S(2)}, u32[]{:S(2)}) collective-permute-start(bf16[2,128,128]{2,1,0:T(8,128)(2,1)S(1)} %get-tuple-element.13), channel_id=1, source_target_pairs={{4,0},{8,4},{12,8},{16,12},{20,16},{24,20},{28,24},{5,1},{9,5},{13... | collective-permute-start | bytes 196616 | tf_op jit(solution)/shard_map/ppermute | solution.py:28
  15.1 2.5 %copy-start.3 = (bf16[512,2048]{1,0:T(8,128)(2,1)S(1)}, bf16[512,2048]{1,0:T(8,128)(2,1)}, u32[]{:S(2)}) copy-start(bf16[512,2048]{1,0:T(8,128)(2,1)} %param.17) | copy-start | bytes 6291460
  15.1 3.0 %copy-start.9 = (bf16[2048,256]{1,0:T(8,128)(2,1)S(1)}, bf16[2048,256]{1,0:T(8,128)(2,1)}, u32[]{:S(2)}) copy-start(bf16[2048,256]{1,0:T(8,128)(2,1)} %param.19) | copy-start | bytes 3145732
  18.1 1.0 copy-start.8
  18.1 1.2 copy-start.4
  18.1 1.5 %copy-start.5 = (f32[384,2]{0,1:T(2,128)S(1)}, f32[384,2]{0,1:T(2,128)}, u32[]{:S(2)}) copy-start(f32[384,2]{0,1:T(2,128)} %param.30) | copy-start | bytes 9220
  18.1 1.6 %copy-start.6 = (f32[384]{0:T(512)S(1)}, f32[384]{0:T(512)}, u32[]{:S(2)}) copy-start(f32[384]{0:T(512)} %param.29) | copy-start | bytes 4612
  19.2 7.7 %copy-start.11 = (f32[4]{0:T(128)S(1)}, f32[4]{0:T(128)}, u32[]{:S(2)}) copy-start(f32[4]{0:T(128)} %param.24) | copy-start | bytes 52
  28.5 2.7 %copy-start.1 = (f32[2,768,512,2]{2,1,3,0:T(8,128)}, f32[2,768,512,2]{2,1,3,0:T(8,128)S(1)}, u32[]{:S(2)}) copy-start(f32[2,768,512,2]{2,1,3,0:T(8,128)S(1)} %get-tuple-element.23) | copy-start | bytes 18874372

commit v2 on v1

--- a/solution.py
+++ b/solution.py
@@ -69,9 +69,15 @@
     return total
 
 
+def turn(p, count):
+    half = count // 2
+    return jnp.where(p == 0, 0, jnp.where(p <= half, p + half - 1, p - half))
+
+
 def exchange_kernel(
     n_ep,
-    send_ref,
+    pick_ref,
+    normed_ref,
     gate_ref,
     up_ref,
     down_ref,
@@ -79,6 +85,8 @@
     attn_ref,
     out_ref,
     attn_out_ref,
+    send_own,
+    send_other,
     rows_buf,
     part_out,
     part_keep,
@@ -92,8 +100,8 @@
     attn_in,
     attn_y_out,
     attn_y_in,
-    local_sem,
     d_send, d_recv,
+    e_send, e_recv,
     p_send, p_recv,
     y_send, y_recv,
     r_send, r_recv,
@@ -109,7 +117,8 @@
     other_core, other_side = 1 - core, 1 - side
     partner = 2 * side + other_core
     across = 2 * other_side + core
-    width = send_ref.shape[2]
+    capacity, width = send_own.shape[1:]
+    half = n_ep // 2
 
     barrier = pltpu.get_barrier_semaphore()
 
@@ -136,7 +145,11 @@
 
     def dispatch(k):
         dest = flip(me, k, n_ep)
-        return remote(send_ref.at[dest], rows_buf.at[lane, k], d_send, d_recv, k, dest, lane)
+        return remote(send_own.at[k], rows_buf.at[lane, k], d_send, d_recv, k, dest, lane)
+
+    def dispatch_other(k):
+        dest = flip(me, k, n_ep)
+        return remote(send_other.at[k], rows_buf.at[across, k], e_send, e_recv, k, dest, lane)
 
     def to_partner(k):
         block = rows_buf.at[lane, k]
@@ -167,33 +180,62 @@
     def attn_side():
         return remote(attn_y_out, attn_y_in, a_send, a_recv, 2, me, across)
 
-    own = pltpu.make_async_copy(send_ref.at[me], rows_buf.at[lane, 0], local_sem)
-    own.start()
-
-    def start_dispatch(k, carry):
+    def gathered(k, quarter):
+        start = pl.multiple_of(quarter * width, width)
+        rows = jnp.dot(
+            pick_ref[flip(me, k, n_ep)],
+            normed_ref[:, pl.ds(start, width)],
+            preferred_element_type=jnp.float32,
+        )
+        return rows.astype(jnp.bfloat16)
+
+    def start_dispatch(p, carry):
+        k = turn(p, n_ep)
+        send_own[k] = gathered(k, lane)
         dispatch(k).start()
+
+        @pl.when(k < half)
+        def _():
+            send_other[k] = gathered(k, across)
+            dispatch_other(k).start()
+
         return carry
 
     lax.fori_loop(1, n_ep, start_dispatch, 0)
+    rows_buf[lane, 0] = gathered(0, lane)
+    rows_buf[across, 0] = gathered(0, across)
     attn_core(0).start()
     attn_core(1).start()
     total[...] = jnp.zeros_like(total)
-    own.wait()
 
     def step(t, carry):
         @pl.when(t < n_ep)
         def _():
-            @pl.when(t > 0)
-            def _():
-                dispatch(t).wait_recv()
-
-            to_partner(t).start()
-            to_across(t).start()
-
-        k5 = t - 3
-
-        @pl.when((k5 >= 0) & (k5 < n_ep))
-        def _():
+            k0 = turn(t, n_ep)
+
+            @pl.when(k0 > 0)
+            def _():
+                dispatch(k0).wait_recv()
+
+            to_partner(k0).start()
+
+            @pl.when(k0 >= half)
+            def _():
+                to_across(k0).start()
+
+            @pl.when((k0 > 0) & (k0 < half))
+            def _():
+                dispatch_other(k0).wait_recv()
+
+            @pl.when(k0 < half)
+            def _():
+                relay(k0).start()
+
+        p5 = t - 3
+
+        @pl.when((p5 >= 0) & (p5 < n_ep))
+        def _():
+            k5 = turn(p5, n_ep)
             sum_core(k5).wait_recv()
             y_out[k5] = (
                 part_keep[k5, other_side].astype(jnp.float32)
@@ -204,20 +246,25 @@
                 jnp.float32
             )
 
-        k1 = t - 1
-
-        @pl.when((k1 >= 0) & (k1 < n_ep))
-        def _():
-            to_across(k1).wait_recv()
-            relay(k1).start()
-
-        k2 = t - 2
-
-        @pl.when((k2 >= 0) & (k2 < n_ep))
-        def _():
+        p1 = t - 1
+
+        @pl.when((p1 >= 0) & (p1 < n_ep))
+        def _():
+            k1 = turn(p1, n_ep)
+
+            @pl.when(k1 >= half)
+            def _():
+                to_across(k1).wait_recv()
+                relay(k1).start()
+
+        p2 = t - 2
+
+        @pl.when((p2 >= 0) & (p2 < n_ep))
+        def _():
+            k2 = turn(p2, n_ep)
             to_partner(k2).wait_recv()
             relay(k2).wait_recv()
-            gate = jnp.zeros((send_ref.shape[1], gate_ref.shape[1]), jnp.float32)
+            gate = jnp.zeros((capacity, gate_ref.shape[1]), jnp.float32)
             up = gate
             for q in range(4):
                 rows = rows_buf[q, k2]
@@ -233,10 +280,11 @@
                     ).astype(jnp.bfloat16)
             sum_core(k2).start()
 
-        k6 = t - 4
-
-        @pl.when((k6 >= 0) & (k6 < n_ep))
-        def _():
+        p6 = t - 4
+
+        @pl.when((p6 >= 0) & (p6 < n_ep))
+        def _():
+            k6 = turn(p6, n_ep)
             sum_side(k6).wait_recv()
             final[k6] = (y_own[k6] + y_in[k6].astype(jnp.float32)).astype(jnp.bfloat16)
 
@@ -248,16 +296,17 @@
             def _():
                 total[...] += jnp.dot(mix_ref[me], final[0], preferred_element_type=jnp.float32)
 
-        k7 = t - 6
-
-        @pl.when((k7 > 0) & (k7 < n_ep))
-        def _():
+        p7 = t - 6
+
+        @pl.when((p7 > 0) & (p7 < n_ep))
+        def _():
+            k7 = turn(p7, n_ep)
             give_back(k7).wait_recv()
             total[...] += jnp.dot(
                 mix_ref[flip(me, k7, n_ep)], back[k7], preferred_element_type=jnp.float32
             )
 
-        @pl.when(t == 1)
+        @pl.when(t == n_ep)
         def _():
             attn_core(0).wait_recv()
             attn_core(1).wait_recv()
@@ -285,7 +334,14 @@
             give_back(k).wait_send()
 
         to_partner(k).wait_send()
-        to_across(k).wait_send()
+        @pl.when(k >= half)
+        def _():
+            to_across(k).wait_send()
+
+        @pl.when((k > 0) & (k < half))
+        def _():
+            dispatch_other(k).wait_send()
+
         relay(k).wait_send()
         sum_core(k).wait_send()
         sum_side(k).wait_send()
@@ -379,7 +435,6 @@
     capacity = max(2, (3 * moe_rows * top_count + 2 * n_ep - 1) // (2 * n_ep))
     moe_normed = rms_scale(x_experts, expert_gain)
     col_width = model_width // tp_count
-    own_cols = lax.dynamic_slice_in_dim(moe_normed, lax.axis_index("tp") * col_width, col_width, 1)
     route_weight = group_prob[:, None] * expert_prob / jnp.sum(expert_prob, axis=1, keepdims=True)
     names = jnp.arange(n_ep, dtype=jnp.int32)
     chosen = routes[:, :, None] == names[None, None, :]
@@ -391,10 +446,6 @@
     share = jnp.sum(jnp.where(chosen, route_weight[:, :, None], 0.0), axis=1)
     slots = jnp.arange(capacity, dtype=jnp.int32)
     pick = (rank.T[:, None, :] == slots[None, :, None]).astype(jnp.bfloat16)
-    outgoing = jnp.dot(
-        pick.reshape(n_ep * capacity, moe_rows), own_cols, preferred_element_type=jnp.float32
-    )
-    outgoing = outgoing.astype(jnp.bfloat16).reshape(n_ep, capacity, col_width)
     mix = jnp.where(
         rank.T[:, :, None] == slots[None, None, :], share.T[:, :, None], 0.0
     ).astype(jnp.bfloat16)
@@ -409,9 +460,11 @@
             jax.ShapeDtypeStruct((moe_rows, col_width), bf16),
             jax.ShapeDtypeStruct((slice_rows, model_width), bf16),
         ),
-        in_specs=[vmem] * 6,
+        in_specs=[vmem] * 7,
         out_specs=(vmem, vmem),
         scratch_shapes=[
+            pltpu.VMEM((n_ep, capacity, col_width), bf16),
+            pltpu.VMEM((n_ep // 2, capacity, col_width), bf16),
             pltpu.VMEM((tp_count, n_ep, capacity, col_width), bf16),
             pltpu.VMEM((n_ep, 2, capacity, col_width), bf16),
             pltpu.VMEM((n_ep, 2, capacity, col_width), bf16),
@@ -425,14 +478,13 @@
             pltpu.VMEM((2, slice_rows, model_width), bf16),
             pltpu.VMEM((slice_rows, model_width), bf16),
             pltpu.VMEM((slice_rows, model_width), bf16),
-            dma(()),
         ]
-        + [dma((n_ep,))] * 14
+        + [dma((n_ep,))] * 16
         + [dma((3,))] * 2,
         compiler_params=pltpu.CompilerParams(
             collective_id=0, has_side_effects=True, vmem_limit_bytes=60 * 1024 * 1024
         ),
-    )(outgoing, w_gate[0], w_up[0], w_down[0], mix, attn_part)
+    )(pick, moe_normed, w_gate[0], w_up[0], w_down[0], mix, attn_part)
     return (attend_out, expert_out)
 
 

time: 132 us -> 133 us (level)
  other arithmetic: 10.2 us -> 14.2 us
  matrix products: 17.5 us -> 14.9 us
  local copies, waits for them, and re-layouts: 6.86 us -> 5.43 us
  Pallas kernels: 88.5 us -> 89.9 us
    dot_general x1 -> x0, matrix products: 3.13 us -> none  [per_device(): jnp.dot(pick.reshape(n_ep * capacity, moe_rows), own_cols, preferred_elem...]
    pallas_call x1, Pallas kernels: 88.5 us -> 89.9 us  [per_device(): pl.pallas_call(functools.partial(exchange_kernel, n_ep), out_shape=(jax.S...]
    convert_element_type x1 -> x2, other arithmetic: 2.04 us -> 2.72 us  [the longest x1 1.57 us: rms_scale(): return (scaled * gain).astype(jnp.bfloat16)]
    unnamed x26 -> x28, local copies, waits for them, and re-layouts: 5.45 us -> 4.91 us
  transfers between devices with their start and end apart: 2 -> 2, of which waited for: 0 -> 0; matrix products, arithmetic and copies ran while one was open for 9% -> 8% of each run, Pallas kernels for 0% -> 0%
where the time goes in v2:
time: 133 us; the launch traced here: 132 us
  Pallas kernels  89.9 us (68%)
  matrix products  14.9 us (11%)
  other arithmetic  14.2 us (11%)
  starting transfers between devices  6.95 us (5%)
  local copies, waits for them, and re-layouts  5.43 us (4%)
    pallas_call x1, Pallas kernels, per_device(): pl.pallas_call(functools.partial(exchange_kernel, n_ep), out_shape=(jax.S...  89.9 us
    ppermute x1, starting transfers between devices, extended(): before = lax.ppermute(last, axis, up)  5.49 us
    unnamed x28, local copies, waits for them, and re-layouts  4.91 us
    dot_general x1, matrix products, per_device(): jnp.einsum('hgqk,khd->qhgd', probs, span_values, preferred_element_type=j...  4.7 us
    dot_general x1, matrix products, per_device(): jnp.dot(normed, w_key, preferred_element_type=jnp.float32)  2.74 us
  transfers between devices with their start and end apart: 2, of which 0 were waited for; matrix products, arithmetic and copies ran while one was open for 8% of the time, Pallas kernels for 0%

profile of v2, /device:TPU:0, one launch (start us, length us, event | category | flops | bytes accessed | tf_op | source)
XLA Modules:
  0.0 132.4 jit_solution(701053701622343491)
XLA Ops:
  0.7 2.2 %fusion.2 = f32[512]{0:T(512)S(1)} fusion(bf16[512,2048]{1,0:T(8,128)(2,1)} %param.17), kind=kLoop, calls=%fused_computation.7 | loop fusion | flops 3145216 | bytes 2099200 | tf_op jit(solution)/shard_map/reduce_sum | solution.py:35
  2.9 2.7 %multiply_reduce_fusion.1 = (f32[512,2]{0,1:T(2,128)S(1)}, f32[512,128]{0,1:T(8,128)S(1)}) fusion(bf16[2048,128]{1,0:T(8,128)(2,1)} %param.20, bf16[512,2048]{1,0:T(8,128)(2,1)} %param.17, f32[2048]{0:T(1024)} %param.18, f32[512]{0:T(512)S(1)} %add_rsqrt_fusion.2), kind=kOutput, calls=%fused_computation.40 | convolution fusion | flops 272759808 | bytes 2897920 | tf_op jit(solution)/shard_map/dot_general | solution.py:393
  5.7 0.2 fusion.20
  6.0 0.1 multiply_multiply_fusion.1
  6.2 0.1 copy.31
  6.3 1.8 %fusion.13 = bf16[1,512,128]{2,1,0:T(8,128)(2,1)S(1)} fusion(bf16[2048,128]{1,0:T(8,128)(2,1)} %param.21, bf16[512,2048]{1,0:T(8,128)(2,1)S(1)} %copy-done.3, f32[2048]{0:T(1024)S(1)} %copy-done.11, f32[512]{0:T(512)S(1)} %add_rsqrt_fusion.2), kind=kOutput, calls=%fused_computation.26 | convolution fusion | flops 272695296 | bytes 2762752 | tf_op jit(solution)/shard_map/dot_general | solution.py:400
  8.1 0.7 pad_maximum_fusion.3
  8.8 5.5 %collective-permute-start = (bf16[2,128,128]{2,1,0:T(8,128)(2,1)}, bf16[2,128,128]{2,1,0:T(8,128)(2,1)}, u32[]{:S(2)}, u32[]{:S(2)}) collective-permute-start(bf16[2,128,128]{2,1,0:T(8,128)(2,1)} %get-tuple-element.12), channel_id=1, source_target_pairs={{0,4},{4,8},{8,12},{12,16},{16,20},{20,24},{24,28},{1,5},{5,9},{9,... | collective-permute-start | bytes 196616 | tf_op jit(solution)/shard_map/ppermute | solution.py:27
  14.3 1.5 %collective-permute-start.1 = (bf16[2,128,128]{2,1,0:T(8,128)(2,1)}, bf16[2,128,128]{2,1,0:T(8,128)(2,1)}, u32[]{:S(2)}, u32[]{:S(2)}) collective-permute-start(bf16[2,128,128]{2,1,0:T(8,128)(2,1)} %get-tuple-element.13), channel_id=1, source_target_pairs={{4,0},{8,4},{12,8},{16,12},{20,16},{24,20},{28,24},{5,1},{9,5},{13... | collective-permute-start | bytes 196616 | tf_op jit(solution)/shard_map/ppermute | solution.py:28
  15.7 0.6 fusion.22
  16.3 2.2 %multiply_reduce_fusion = (f32[512,4]{0,1:T(4,128)S(1)}, f32[512,256]{0,1:T(8,128)S(1)}) fusion(bf16[2048,256]{1,0:T(8,128)(2,1)} %param.19, bf16[512,2048]{1,0:T(8,128)(2,1)S(1)} %copy-done.3, f32[2048]{0:T(1024)} %param.18, f32[512]{0:T(512)} %copy-done.9), kind=kOutput, calls=%fused_computation.31 | convolution fusion | flops 541325312 | bytes 3688448 | tf_op jit(solution)/shard_map/dot_general | solution.py:385
  18.6 0.9 multiply_multiply_fusion
  19.4 0.1 subtract_convert_fusion
  19.6 0.1 fusion.14
  19.8 0.7 multiply_divide_fusion
  20.5 1.2 fusion.9.pick_ref
  21.6 2.3 %select_convert_fusion.mix_ref = bf16[8,384,144]{2,1,0:T(8,128)(2,1)} fusion(bf16[8,384]{1,0:T(8,128)(2,1)S(1)} %bitcast.60, s32[8,384]{1,0:T(8,128)S(1)} %fusion.14), kind=kLoop, calls=%fused_computation.15 | loop fusion | flops 884736 | bytes 903168 | tf_op jit(solution)/shard_map/convert_element_type | solution.py:451
  24.0 0.4 fusion.5
  24.4 1.6 %fusion.7.normed_ref = bf16[384,2048]{1,0:T(8,128)(2,1)} fusion(bf16[384,2048]{1,0:T(8,128)(2,1)S(1)} %copy-done.2, f32[2048]{0:T(1024)S(1)} %copy-done.6, f32[384]{0:T(512)S(1)} %add_rsqrt_fusion.3), kind=kLoop, calls=%fused_computation.14 | loop fusion | flops 3145728 | bytes 3155456 | tf_op jit(solution)/shard_map/convert_element_type | solution.py:36
  26.0 0.7 fusion.11
  26.7 0.1 max.17
  26.8 0.9 pad_maximum_fusion
  27.7 0.1 copy.33
  27.9 1.3 fusion.1
  29.3 1.4 %fusion = f32[2,2,512]{2,1,0:T(2,128)S(1)} fusion(f32[2,768,512,2]{2,1,3,0:T(8,128)S(1)} %get-tuple-element.23, f32[2,2,512]{2,1,0:T(2,128)S(1)} %broadcast_maximum_fusion, pred[512,768]{0,1:T(8,128)(4,1)S(1)} %fusion.11), kind=kLoop, calls=%fused_computation.3 | loop fusion | flops 6289408 | bytes 6701056 | tf_op jit(solution)/shard_map/reduce_sum | solution.py:422
  30.6 1.2 copy-done.1
  31.9 0.1 copy.32
  32.1 4.7 %fusion.12 = bf16[2,64,2,512]{3,1,2,0:T(8,128)(2,1)S(1)} fusion(bf16[768,2,64,1]{0,2,3,1:T(8,128)(2,1)S(1)} %bitcast.57, f32[2,768,512,2]{2,1,3,0:T(8,128)} %copy-done.1, f32[2,2,512]{2,1,0:T(2,128)S(1)} %exponential_add_fusion, f32[2,2,512]{2,1,0:T(2,128)S(1)} %broadcast_maximum_fusion, pred[512,768]{0,1:T(8,128)(4,1)S(1)} %fusion.11), kind=kOutput, calls=%fused_computation.24 | convolution fusion | flops 209321984 | bytes 7159808 | tf_op jit(solution)/shard_map/hgqk,khd->qhgd/dot_general | solution.py:424
  36.8 2.1 %convolution_convert_fusion = bf16[512,2048]{1,0:T(8,128)(2,1)} fusion(bf16[512,256]{0,1:T(8,128)(2,1)S(1)} %bitcast.54, bf16[256,2048]{1,0:T(8,128)(2,1)S(1)} %copy-done), kind=kOutput, calls=%fused_computation.18 | convolution fusion | flops 537919488 | bytes 3407872 | tf_op jit(solution)/shard_map/dot_general | solution.py:428
  38.9 89.9 %shard_map.176 = (bf16[384,512]{1,0:T(8,128)(2,1)}, bf16[128,2048]{1,0:T(8,128)(2,1)}) custom-call(bf16[8,144,384]{2,1,0:T(8,128)(2,1)} %fusion.9.pick_ref, bf16[384,2048]{1,0:T(8,128)(2,1)} %fusion.7.normed_ref, bf16[2048,256]{1,0:T(8,128)(2,1)} %bitcast.51, bf16[2048,256]{1,0:T(8,128)(2,1)} %bitcast.52, bf16[256,2048]{1,0:T(8,128)(2,1)} %bitcast.53, ...), custom_call_target="tpu_custom_call" | custom-call | tf_op jit(solution)/shard_map/pallas_call | solution.py:457
  128.7 1.9 %copy.40 = bf16[128,2048]{1,0:T(8,128)(2,1)} copy(bf16[128,2048]{1,0:T(8,128)(2,1)} %get-tuple-element.30) | data formatting | bytes 1048576
  130.6 1.8 %copy.41 = bf16[384,512]{1,0:T(8,128)(2,1)} copy(bf16[384,512]{1,0:T(8,128)(2,1)} %get-tuple-element.31) | data formatting | bytes 786432
  (44 shorter events, 0.5 us)
Async XLA Ops:
  0.6 36.1 %copy-start = (bf16[256,2048]{1,0:T(8,128)(2,1)S(1)}, bf16[256,2048]{1,0:T(8,128)(2,1)}, u32[]{:S(2)}) copy-start(bf16[256,2048]{1,0:T(8,128)(2,1)} %param.25) | copy-start | bytes 3145732
  0.7 5.3 %copy-start.10 = (f32[64]{0:T(128)S(1)}, f32[64]{0:T(128)}, u32[]{:S(2)}) copy-start(f32[64]{0:T(128)} %param.23) | copy-start | bytes 772
  2.9 3.4 %copy-start.3 = (bf16[512,2048]{1,0:T(8,128)(2,1)S(1)}, bf16[512,2048]{1,0:T(8,128)(2,1)}, u32[]{:S(2)}) copy-start(bf16[512,2048]{1,0:T(8,128)(2,1)} %param.17) | copy-start | bytes 6291460
  2.9 3.4 %copy-start.11 = (f32[2048]{0:T(1024)S(1)}, f32[2048]{0:T(1024)}, u32[]{:S(2)}) copy-start(f32[2048]{0:T(1024)} %param.18) | copy-start | bytes 24580
  2.9 5.2 %copy-start.9 = (f32[512]{0:T(512)}, f32[512]{0:T(512)S(1)}, u32[]{:S(2)}) copy-start(f32[512]{0:T(512)S(1)} %add_rsqrt_fusion.2) | copy-start | bytes 6148
  8.8 18.0 %collective-permute-start = (bf16[2,128,128]{2,1,0:T(8,128)(2,1)}, bf16[2,128,128]{2,1,0:T(8,128)(2,1)}, u32[]{:S(2)}, u32[]{:S(2)}) collective-permute-start(bf16[2,128,128]{2,1,0:T(8,128)(2,1)} %get-tuple-element.12), channel_id=1, source_target_pairs={{0,4},{4,8},{8,12},{12,16},{16,20},{20,24},{24,28},{1,5},{5,9},{9,... | collective-permute-start | bytes 196616 | tf_op jit(solution)/shard_map/ppermute | solution.py:27
  14.3 12.5 %collective-permute-start.1 = (bf16[2,128,128]{2,1,0:T(8,128)(2,1)}, bf16[2,128,128]{2,1,0:T(8,128)(2,1)}, u32[]{:S(2)}, u32[]{:S(2)}) collective-permute-start(bf16[2,128,128]{2,1,0:T(8,128)(2,1)} %get-tuple-element.13), channel_id=1, source_target_pairs={{4,0},{8,4},{12,8},{16,12},{20,16},{24,20},{28,24},{5,1},{9,5},{13... | collective-permute-start | bytes 196616 | tf_op jit(solution)/shard_map/ppermute | solution.py:28
  16.3 3.2 %copy-start.4 = (s32[384,2]{0,1:T(2,128)S(1)}, s32[384,2]{0,1:T(2,128)}, u32[]{:S(2)}) copy-start(s32[384,2]{0,1:T(2,128)} %param.28) | copy-start | bytes 9220
  16.3 3.4 %copy-start.5 = (f32[384,2]{0,1:T(2,128)S(1)}, f32[384,2]{0,1:T(2,128)}, u32[]{:S(2)}) copy-start(f32[384,2]{0,1:T(2,128)} %param.30) | copy-start | bytes 9220
  18.5 5.5 %copy-start.2 = (bf16[384,2048]{1,0:T(8,128)(2,1)S(1)}, bf16[384,2048]{1,0:T(8,128)(2,1)}, u32[]{:S(2)}) copy-start(bf16[384,2048]{1,0:T(8,128)(2,1)} %param.26) | copy-start | bytes 4718596
  18.5 5.8 %copy-start.6 = (f32[2048]{0:T(1024)S(1)}, f32[2048]{0:T(1024)}, u32[]{:S(2)}) copy-start(f32[2048]{0:T(1024)} %param.27) | copy-start | bytes 24580
  21.6 4.3 %copy-start.7 = (pred[768]{0:T(1024)(128)(4,1)S(1)}, pred[768]{0:T(1024)(128)(4,1)}, u32[]{:S(2)}) copy-start(pred[768]{0:T(1024)(128)(4,1)} %get-tuple-element.26) | copy-start | bytes 2308
  21.6 4.3 %copy-start.8 = (pred[768]{0:T(1024)(128)(4,1)S(1)}, pred[768]{0:T(1024)(128)(4,1)}, u32[]{:S(2)}) copy-start(pred[768]{0:T(1024)(128)(4,1)} %get-tuple-element.27) | copy-start | bytes 2308
  21.6 5.1 %copy-start.12 = (f32[4]{0:T(128)S(1)}, f32[4]{0:T(128)}, u32[]{:S(2)}) copy-start(f32[4]{0:T(128)} %param.24) | copy-start | bytes 52
  29.2 2.7 %copy-start.1 = (f32[2,768,512,2]{2,1,3,0:T(8,128)}, f32[2,768,512,2]{2,1,3,0:T(8,128)S(1)}, u32[]{:S(2)}) copy-start(f32[2,768,512,2]{2,1,3,0:T(8,128)S(1)} %get-tuple-element.23) | copy-start | bytes 18874372

commit v3 on v2

--- a/solution.py
+++ b/solution.py
@@ -231,7 +231,7 @@
             def _():
                 relay(k0).start()
 
-        p5 = t - 3
+        p5 = t - 4
 
         @pl.when((p5 >= 0) & (p5 < n_ep))
         def _():
@@ -246,7 +246,7 @@
                 jnp.float32
             )
 
-        p1 = t - 1
+        p1 = t - 2
 
         @pl.when((p1 >= 0) & (p1 < n_ep))
         def _():
@@ -257,7 +257,7 @@
                 to_across(k1).wait_recv()
                 relay(k1).start()
 
-        p2 = t - 2
+        p2 = t - 3
 
         @pl.when((p2 >= 0) & (p2 < n_ep))
         def _():
@@ -280,7 +280,7 @@
                     ).astype(jnp.bfloat16)
             sum_core(k2).start()
 
-        p6 = t - 4
+        p6 = t - 6
 
         @pl.when((p6 >= 0) & (p6 < n_ep))
         def _():
@@ -296,7 +296,7 @@
             def _():
                 total[...] += jnp.dot(mix_ref[me], final[0], preferred_element_type=jnp.float32)
 
-        p7 = t - 6
+        p7 = t - 9
 
         @pl.when((p7 > 0) & (p7 < n_ep))
         def _():
@@ -306,7 +306,7 @@
                 mix_ref[flip(me, k7, n_ep)], back[k7], preferred_element_type=jnp.float32
             )
 
-        @pl.when(t == n_ep)
+        @pl.when(t == 0)
         def _():
             attn_core(0).wait_recv()
             attn_core(1).wait_recv()
@@ -318,7 +318,7 @@
 
         return carry
 
-    lax.fori_loop(0, n_ep + 6, step, 0)
+    lax.fori_loop(0, n_ep + 9, step, 0)
     attn_side().wait_recv()
     attn_out_ref[...] = (
         attn_ref[2 * side + core].astype(jnp.float32)

time: 133 us -> 123 us (0.925)
  Pallas kernels: 89.9 us -> 80.4 us
    pallas_call x1, Pallas kernels: 89.9 us -> 80.4 us  [per_device(): pl.pallas_call(functools.partial(exchange_kernel, n_ep), out_shape=(jax.S...]
  transfers between devices with their start and end apart: 2 -> 2, of which waited for: 0 -> 0; matrix products, arithmetic and copies ran while one was open for 8% -> 9% of each run, Pallas kernels for 0% -> 0%
where the time goes in v3:
time: 123 us
  Pallas kernels  80.4 us (65%)
  matrix products  14.9 us (12%)
  other arithmetic  14.2 us (12%)
  starting transfers between devices  6.95 us (6%)
  local copies, waits for them, and re-layouts  5.43 us (4%)
    pallas_call x1, Pallas kernels, per_device(): pl.pallas_call(functools.partial(exchange_kernel, n_ep), out_shape=(jax.S...  80.4 us
    ppermute x1, starting transfers between devices, extended(): before = lax.ppermute(last, axis, up)  5.49 us
    unnamed x28, local copies, waits for them, and re-layouts  4.91 us
    dot_general x1, matrix products, per_device(): jnp.einsum('hgqk,khd->qhgd', probs, span_values, preferred_element_type=j...  4.7 us
    dot_general x1, matrix products, per_device(): jnp.dot(normed, w_key, preferred_element_type=jnp.float32)  2.74 us
    reduce_sum x2, other arithmetic, rms_scale(): jnp.mean(values_f * values_f, axis=-1, keepdims=True) + epsilon  2.54 us
  transfers between devices with their start and end apart: 2, of which 0 were waited for; matrix products, arithmetic and copies ran while one was open for 9% of the time, Pallas kernels for 0%

profile of v3, /device:TPU:0, one launch (start us, length us, event | category | flops | bytes accessed | tf_op | source)
XLA Modules:
  0.0 122.9 jit_solution(16635669474047097471)
XLA Ops:
  0.7 2.2 %fusion.2 = f32[512]{0:T(512)S(1)} fusion(bf16[512,2048]{1,0:T(8,128)(2,1)} %param.17), kind=kLoop, calls=%fused_computation.7 | loop fusion | flops 3145216 | bytes 2099200 | tf_op jit(solution)/shard_map/reduce_sum | solution.py:35
  2.9 2.7 %multiply_reduce_fusion.1 = (f32[512,2]{0,1:T(2,128)S(1)}, f32[512,128]{0,1:T(8,128)S(1)}) fusion(bf16[2048,128]{1,0:T(8,128)(2,1)} %param.20, bf16[512,2048]{1,0:T(8,128)(2,1)} %param.17, f32[2048]{0:T(1024)} %param.18, f32[512]{0:T(512)S(1)} %add_rsqrt_fusion.2), kind=kOutput, calls=%fused_computation.40 | convolution fusion | flops 272759808 | bytes 2897920 | tf_op jit(solution)/shard_map/dot_general | solution.py:393
  5.7 0.2 fusion.20
  6.0 0.1 multiply_multiply_fusion.1
  6.2 0.1 copy.31
  6.3 1.8 %fusion.13 = bf16[1,512,128]{2,1,0:T(8,128)(2,1)S(1)} fusion(bf16[2048,128]{1,0:T(8,128)(2,1)} %param.21, bf16[512,2048]{1,0:T(8,128)(2,1)S(1)} %copy-done.3, f32[2048]{0:T(1024)S(1)} %copy-done.11, f32[512]{0:T(512)S(1)} %add_rsqrt_fusion.2), kind=kOutput, calls=%fused_computation.26 | convolution fusion | flops 272695296 | bytes 2762752 | tf_op jit(solution)/shard_map/dot_general | solution.py:400
  8.1 0.7 pad_maximum_fusion.3
  8.8 5.5 %collective-permute-start = (bf16[2,128,128]{2,1,0:T(8,128)(2,1)}, bf16[2,128,128]{2,1,0:T(8,128)(2,1)}, u32[]{:S(2)}, u32[]{:S(2)}) collective-permute-start(bf16[2,128,128]{2,1,0:T(8,128)(2,1)} %get-tuple-element.12), channel_id=1, source_target_pairs={{0,4},{4,8},{8,12},{12,16},{16,20},{20,24},{24,28},{1,5},{5,9},{9,... | collective-permute-start | bytes 196616 | tf_op jit(solution)/shard_map/ppermute | solution.py:27
  14.3 1.5 %collective-permute-start.1 = (bf16[2,128,128]{2,1,0:T(8,128)(2,1)}, bf16[2,128,128]{2,1,0:T(8,128)(2,1)}, u32[]{:S(2)}, u32[]{:S(2)}) collective-permute-start(bf16[2,128,128]{2,1,0:T(8,128)(2,1)} %get-tuple-element.13), channel_id=1, source_target_pairs={{4,0},{8,4},{12,8},{16,12},{20,16},{24,20},{28,24},{5,1},{9,5},{13... | collective-permute-start | bytes 196616 | tf_op jit(solution)/shard_map/ppermute | solution.py:28
  15.7 0.6 fusion.22
  16.3 2.2 %multiply_reduce_fusion = (f32[512,4]{0,1:T(4,128)S(1)}, f32[512,256]{0,1:T(8,128)S(1)}) fusion(bf16[2048,256]{1,0:T(8,128)(2,1)} %param.19, bf16[512,2048]{1,0:T(8,128)(2,1)S(1)} %copy-done.3, f32[2048]{0:T(1024)} %param.18, f32[512]{0:T(512)} %copy-done.9), kind=kOutput, calls=%fused_computation.31 | convolution fusion | flops 541325312 | bytes 3688448 | tf_op jit(solution)/shard_map/dot_general | solution.py:385
  18.6 0.9 multiply_multiply_fusion
  19.4 0.1 subtract_convert_fusion
  19.6 0.1 fusion.14
  19.8 0.7 multiply_divide_fusion
  20.5 1.2 fusion.9.pick_ref
  21.6 2.3 %select_convert_fusion.mix_ref = bf16[8,384,144]{2,1,0:T(8,128)(2,1)} fusion(bf16[8,384]{1,0:T(8,128)(2,1)S(1)} %bitcast.60, s32[8,384]{1,0:T(8,128)S(1)} %fusion.14), kind=kLoop, calls=%fused_computation.15 | loop fusion | flops 884736 | bytes 903168 | tf_op jit(solution)/shard_map/convert_element_type | solution.py:451
  24.0 0.4 fusion.5
  24.4 1.6 %fusion.7.normed_ref = bf16[384,2048]{1,0:T(8,128)(2,1)} fusion(bf16[384,2048]{1,0:T(8,128)(2,1)S(1)} %copy-done.2, f32[2048]{0:T(1024)S(1)} %copy-done.6, f32[384]{0:T(512)S(1)} %add_rsqrt_fusion.3), kind=kLoop, calls=%fused_computation.14 | loop fusion | flops 3145728 | bytes 3155456 | tf_op jit(solution)/shard_map/convert_element_type | solution.py:36
  26.0 0.7 fusion.11
  26.7 0.1 max.17
  26.8 0.9 pad_maximum_fusion
  27.7 0.1 copy.33
  27.9 1.3 %fusion.1 = (f32[2,2,512]{2,1,0:T(2,128)S(1)}, f32[2,768,512,2]{2,1,3,0:T(8,128)S(1)}) fusion(pred[512,768]{0,1:T(8,128)(4,1)S(1)} %fusion.11, bf16[768,2,64,1]{0,2,3,1:T(8,128)(2,1)S(1)} %bitcast.56, bf16[512,2,2,32]{0,3,2,1:T(8,128)(2,1)S(1)} %bitcast.59, bf16[512,2,2,32]{0,3,2,1:T(8,128)(2,1)S(1)} %bitcast.58), kind=kOutput, calls=%fused_computation.6 | convolution fusion | flops 206567424 | bytes 7151616 | tf_op jit(solution)/shard_map/qhgd,khd->hgqk/dot_general | solution.py:405
  29.3 1.4 %fusion = f32[2,2,512]{2,1,0:T(2,128)S(1)} fusion(f32[2,768,512,2]{2,1,3,0:T(8,128)S(1)} %get-tuple-element.23, f32[2,2,512]{2,1,0:T(2,128)S(1)} %broadcast_maximum_fusion, pred[512,768]{0,1:T(8,128)(4,1)S(1)} %fusion.11), kind=kLoop, calls=%fused_computation.3 | loop fusion | flops 6289408 | bytes 6701056 | tf_op jit(solution)/shard_map/reduce_sum | solution.py:422
  30.6 1.2 copy-done.1
  31.9 0.1 copy.32
  32.1 4.7 %fusion.12 = bf16[2,64,2,512]{3,1,2,0:T(8,128)(2,1)S(1)} fusion(bf16[768,2,64,1]{0,2,3,1:T(8,128)(2,1)S(1)} %bitcast.57, f32[2,768,512,2]{2,1,3,0:T(8,128)} %copy-done.1, f32[2,2,512]{2,1,0:T(2,128)S(1)} %exponential_add_fusion, f32[2,2,512]{2,1,0:T(2,128)S(1)} %broadcast_maximum_fusion, pred[512,768]{0,1:T(8,128)(4,1)S(1)} %fusion.11), kind=kOutput, calls=%fused_computation.24 | convolution fusion | flops 209321984 | bytes 7159808 | tf_op jit(solution)/shard_map/hgqk,khd->qhgd/dot_general | solution.py:424
  36.8 2.1 %convolution_convert_fusion = bf16[512,2048]{1,0:T(8,128)(2,1)} fusion(bf16[512,256]{0,1:T(8,128)(2,1)S(1)} %bitcast.54, bf16[256,2048]{1,0:T(8,128)(2,1)S(1)} %copy-done), kind=kOutput, calls=%fused_computation.18 | convolution fusion | flops 537919488 | bytes 3407872 | tf_op jit(solution)/shard_map/dot_general | solution.py:428
  38.9 80.4 %shard_map.176 = (bf16[384,512]{1,0:T(8,128)(2,1)}, bf16[128,2048]{1,0:T(8,128)(2,1)}) custom-call(bf16[8,144,384]{2,1,0:T(8,128)(2,1)} %fusion.9.pick_ref, bf16[384,2048]{1,0:T(8,128)(2,1)} %fusion.7.normed_ref, bf16[2048,256]{1,0:T(8,128)(2,1)} %bitcast.51, bf16[2048,256]{1,0:T(8,128)(2,1)} %bitcast.52, bf16[256,2048]{1,0:T(8,128)(2,1)} %bitcast.53, ...), custom_call_target="tpu_custom_call" | custom-call | tf_op jit(solution)/shard_map/pallas_call | solution.py:457
  119.2 1.9 %copy.40 = bf16[128,2048]{1,0:T(8,128)(2,1)} copy(bf16[128,2048]{1,0:T(8,128)(2,1)} %get-tuple-element.30) | data formatting | bytes 1048576
  121.1 1.8 %copy.41 = bf16[384,512]{1,0:T(8,128)(2,1)} copy(bf16[384,512]{1,0:T(8,128)(2,1)} %get-tuple-element.31) | data formatting | bytes 786432
  (44 shorter events, 0.5 us)
Async XLA Ops:
  0.6 36.1 %copy-start = (bf16[256,2048]{1,0:T(8,128)(2,1)S(1)}, bf16[256,2048]{1,0:T(8,128)(2,1)}, u32[]{:S(2)}) copy-start(bf16[256,2048]{1,0:T(8,128)(2,1)} %param.25) | copy-start | bytes 3145732
  0.7 5.3 %copy-start.10 = (f32[64]{0:T(128)S(1)}, f32[64]{0:T(128)}, u32[]{:S(2)}) copy-start(f32[64]{0:T(128)} %param.23) | copy-start | bytes 772
  2.9 3.4 %copy-start.3 = (bf16[512,2048]{1,0:T(8,128)(2,1)S(1)}, bf16[512,2048]{1,0:T(8,128)(2,1)}, u32[]{:S(2)}) copy-start(bf16[512,2048]{1,0:T(8,128)(2,1)} %param.17) | copy-start | bytes 6291460
  2.9 3.4 %copy-start.11 = (f32[2048]{0:T(1024)S(1)}, f32[2048]{0:T(1024)}, u32[]{:S(2)}) copy-start(f32[2048]{0:T(1024)} %param.18) | copy-start | bytes 24580
  2.9 5.2 %copy-start.9 = (f32[512]{0:T(512)}, f32[512]{0:T(512)S(1)}, u32[]{:S(2)}) copy-start(f32[512]{0:T(512)S(1)} %add_rsqrt_fusion.2) | copy-start | bytes 6148
  8.8 18.0 %collective-permute-start = (bf16[2,128,128]{2,1,0:T(8,128)(2,1)}, bf16[2,128,128]{2,1,0:T(8,128)(2,1)}, u32[]{:S(2)}, u32[]{:S(2)}) collective-permute-start(bf16[2,128,128]{2,1,0:T(8,128)(2,1)} %get-tuple-element.12), channel_id=1, source_target_pairs={{0,4},{4,8},{8,12},{12,16},{16,20},{20,24},{24,28},{1,5},{5,9},{9,... | collective-permute-start | bytes 196616 | tf_op jit(solution)/shard_map/ppermute | solution.py:27
  14.3 12.5 %collective-permute-start.1 = (bf16[2,128,128]{2,1,0:T(8,128)(2,1)}, bf16[2,128,128]{2,1,0:T(8,128)(2,1)}, u32[]{:S(2)}, u32[]{:S(2)}) collective-permute-start(bf16[2,128,128]{2,1,0:T(8,128)(2,1)} %get-tuple-element.13), channel_id=1, source_target_pairs={{4,0},{8,4},{12,8},{16,12},{20,16},{24,20},{28,24},{5,1},{9,5},{13... | collective-permute-start | bytes 196616 | tf_op jit(solution)/shard_map/ppermute | solution.py:28
  16.3 3.2 %copy-start.4 = (s32[384,2]{0,1:T(2,128)S(1)}, s32[384,2]{0,1:T(2,128)}, u32[]{:S(2)}) copy-start(s32[384,2]{0,1:T(2,128)} %param.28) | copy-start | bytes 9220
  16.3 3.4 %copy-start.5 = (f32[384,2]{0,1:T(2,128)S(1)}, f32[384,2]{0,1:T(2,128)}, u32[]{:S(2)}) copy-start(f32[384,2]{0,1:T(2,128)} %param.30) | copy-start | bytes 9220
  18.5 5.5 %copy-start.2 = (bf16[384,2048]{1,0:T(8,128)(2,1)S(1)}, bf16[384,2048]{1,0:T(8,128)(2,1)}, u32[]{:S(2)}) copy-start(bf16[384,2048]{1,0:T(8,128)(2,1)} %param.26) | copy-start | bytes 4718596
  18.5 5.8 %copy-start.6 = (f32[2048]{0:T(1024)S(1)}, f32[2048]{0:T(1024)}, u32[]{:S(2)}) copy-start(f32[2048]{0:T(1024)} %param.27) | copy-start | bytes 24580
  21.6 4.3 %copy-start.7 = (pred[768]{0:T(1024)(128)(4,1)S(1)}, pred[768]{0:T(1024)(128)(4,1)}, u32[]{:S(2)}) copy-start(pred[768]{0:T(1024)(128)(4,1)} %get-tuple-element.26) | copy-start | bytes 2308
  21.6 4.3 %copy-start.8 = (pred[768]{0:T(1024)(128)(4,1)S(1)}, pred[768]{0:T(1024)(128)(4,1)}, u32[]{:S(2)}) copy-start(pred[768]{0:T(1024)(128)(4,1)} %get-tuple-element.27) | copy-start | bytes 2308
  21.6 5.1 %copy-start.12 = (f32[4]{0:T(128)S(1)}, f32[4]{0:T(128)}, u32[]{:S(2)}) copy-start(f32[4]{0:T(128)} %param.24) | copy-start | bytes 52
  29.2 2.7 %copy-start.1 = (f32[2,768,512,2]{2,1,3,0:T(8,128)}, f32[2,768,512,2]{2,1,3,0:T(8,128)S(1)}, u32[]{:S(2)}) copy-start(f32[2,768,512,2]{2,1,3,0:T(8,128)S(1)} %get-tuple-element.23) | copy-start | bytes 18874372

commit v4 on v3

--- a/solution.py
+++ b/solution.py
@@ -70,8 +70,7 @@
 
 
 def turn(p, count):
-    half = count // 2
-    return jnp.where(p == 0, 0, jnp.where(p <= half, p + half - 1, p - half))
+    return p // 2 + lax.rem(p, 2) * (count // 2)
 
 
 def exchange_kernel(

time: 123 us -> 117 us (0.951)
  Pallas kernels: 80.4 us -> 74.5 us
    pallas_call x1, Pallas kernels: 80.4 us -> 74.5 us  [per_device(): pl.pallas_call(functools.partial(exchange_kernel, n_ep), out_shape=(jax.S...]
where the time goes in v4:
time: 117 us
  Pallas kernels  74.5 us (64%)
  matrix products  14.9 us (13%)
  other arithmetic  14.2 us (12%)
  starting transfers between devices  6.95 us (6%)
  local copies, waits for them, and re-layouts  5.43 us (5%)
    pallas_call x1, Pallas kernels, per_device(): pl.pallas_call(functools.partial(exchange_kernel, n_ep), out_shape=(jax.S...  74.5 us
    ppermute x1, starting transfers between devices, extended(): before = lax.ppermute(last, axis, up)  5.49 us
    unnamed x28, local copies, waits for them, and re-layouts  4.91 us
    dot_general x1, matrix products, per_device(): jnp.einsum('hgqk,khd->qhgd', probs, span_values, preferred_element_type=j...  4.7 us
    dot_general x1, matrix products, per_device(): jnp.dot(normed, w_key, preferred_element_type=jnp.float32)  2.74 us
    reduce_sum x2, other arithmetic, rms_scale(): jnp.mean(values_f * values_f, axis=-1, keepdims=True) + epsilon  2.54 us
    convert_element_type x1, other arithmetic, per_device(): mix = jnp.where(rank.T[:, :, None] == slots[None, None, :], share.T[:, :,...  2.34 us
  transfers between devices with their start and end apart: 2, of which 0 were waited for; matrix products, arithmetic and copies ran while one was open for 9% of the time, Pallas kernels for 0%

profile of v4, /device:TPU:0, one launch (start us, length us, event | category | flops | bytes accessed | tf_op | source)
XLA Modules:
  0.0 117.0 jit_solution(10100863075038250670)
XLA Ops:
  0.7 2.2 %fusion.2 = f32[512]{0:T(512)S(1)} fusion(bf16[512,2048]{1,0:T(8,128)(2,1)} %param.17), kind=kLoop, calls=%fused_computation.7 | loop fusion | flops 3145216 | bytes 2099200 | tf_op jit(solution)/shard_map/reduce_sum | solution.py:35
  2.9 2.7 %multiply_reduce_fusion.1 = (f32[512,2]{0,1:T(2,128)S(1)}, f32[512,128]{0,1:T(8,128)S(1)}) fusion(bf16[2048,128]{1,0:T(8,128)(2,1)} %param.20, bf16[512,2048]{1,0:T(8,128)(2,1)} %param.17, f32[2048]{0:T(1024)} %param.18, f32[512]{0:T(512)S(1)} %add_rsqrt_fusion.2), kind=kOutput, calls=%fused_computation.40 | convolution fusion | flops 272759808 | bytes 2897920 | tf_op jit(solution)/shard_map/dot_general | solution.py:392
  5.7 0.2 fusion.20
  6.0 0.1 multiply_multiply_fusion.1
  6.2 0.1 copy.31
  6.3 1.8 %fusion.13 = bf16[1,512,128]{2,1,0:T(8,128)(2,1)S(1)} fusion(bf16[2048,128]{1,0:T(8,128)(2,1)} %param.21, bf16[512,2048]{1,0:T(8,128)(2,1)S(1)} %copy-done.3, f32[2048]{0:T(1024)S(1)} %copy-done.11, f32[512]{0:T(512)S(1)} %add_rsqrt_fusion.2), kind=kOutput, calls=%fused_computation.26 | convolution fusion | flops 272695296 | bytes 2762752 | tf_op jit(solution)/shard_map/dot_general | solution.py:399
  8.1 0.7 pad_maximum_fusion.3
  8.8 5.5 %collective-permute-start = (bf16[2,128,128]{2,1,0:T(8,128)(2,1)}, bf16[2,128,128]{2,1,0:T(8,128)(2,1)}, u32[]{:S(2)}, u32[]{:S(2)}) collective-permute-start(bf16[2,128,128]{2,1,0:T(8,128)(2,1)} %get-tuple-element.12), channel_id=1, source_target_pairs={{0,4},{4,8},{8,12},{12,16},{16,20},{20,24},{24,28},{1,5},{5,9},{9,... | collective-permute-start | bytes 196616 | tf_op jit(solution)/shard_map/ppermute | solution.py:27
  14.3 1.5 %collective-permute-start.1 = (bf16[2,128,128]{2,1,0:T(8,128)(2,1)}, bf16[2,128,128]{2,1,0:T(8,128)(2,1)}, u32[]{:S(2)}, u32[]{:S(2)}) collective-permute-start(bf16[2,128,128]{2,1,0:T(8,128)(2,1)} %get-tuple-element.13), channel_id=1, source_target_pairs={{4,0},{8,4},{12,8},{16,12},{20,16},{24,20},{28,24},{5,1},{9,5},{13... | collective-permute-start | bytes 196616 | tf_op jit(solution)/shard_map/ppermute | solution.py:28
  15.7 0.6 fusion.22
  16.3 2.2 %multiply_reduce_fusion = (f32[512,4]{0,1:T(4,128)S(1)}, f32[512,256]{0,1:T(8,128)S(1)}) fusion(bf16[2048,256]{1,0:T(8,128)(2,1)} %param.19, bf16[512,2048]{1,0:T(8,128)(2,1)S(1)} %copy-done.3, f32[2048]{0:T(1024)} %param.18, f32[512]{0:T(512)} %copy-done.9), kind=kOutput, calls=%fused_computation.31 | convolution fusion | flops 541325312 | bytes 3688448 | tf_op jit(solution)/shard_map/dot_general | solution.py:384
  18.6 0.9 multiply_multiply_fusion
  19.4 0.1 subtract_convert_fusion
  19.6 0.1 fusion.14
  19.8 0.7 multiply_divide_fusion
  20.5 1.2 fusion.9.pick_ref
  21.6 2.3 %select_convert_fusion.mix_ref = bf16[8,384,144]{2,1,0:T(8,128)(2,1)} fusion(bf16[8,384]{1,0:T(8,128)(2,1)S(1)} %bitcast.60, s32[8,384]{1,0:T(8,128)S(1)} %fusion.14), kind=kLoop, calls=%fused_computation.15 | loop fusion | flops 884736 | bytes 903168 | tf_op jit(solution)/shard_map/convert_element_type | solution.py:450
  24.0 0.4 fusion.5
  24.4 1.6 %fusion.7.normed_ref = bf16[384,2048]{1,0:T(8,128)(2,1)} fusion(bf16[384,2048]{1,0:T(8,128)(2,1)S(1)} %copy-done.2, f32[2048]{0:T(1024)S(1)} %copy-done.6, f32[384]{0:T(512)S(1)} %add_rsqrt_fusion.3), kind=kLoop, calls=%fused_computation.14 | loop fusion | flops 3145728 | bytes 3155456 | tf_op jit(solution)/shard_map/convert_element_type | solution.py:36
  26.0 0.7 fusion.11
  26.8 0.9 pad_maximum_fusion
  27.7 0.1 copy.33
  27.9 1.3 %fusion.1 = (f32[2,2,512]{2,1,0:T(2,128)S(1)}, f32[2,768,512,2]{2,1,3,0:T(8,128)S(1)}) fusion(pred[512,768]{0,1:T(8,128)(4,1)S(1)} %fusion.11, bf16[768,2,64,1]{0,2,3,1:T(8,128)(2,1)S(1)} %bitcast.56, bf16[512,2,2,32]{0,3,2,1:T(8,128)(2,1)S(1)} %bitcast.59, bf16[512,2,2,32]{0,3,2,1:T(8,128)(2,1)S(1)} %bitcast.58), kind=kOutput, calls=%fused_computation.6 | convolution fusion | flops 206567424 | bytes 7151616 | tf_op jit(solution)/shard_map/qhgd,khd->hgqk/dot_general | solution.py:404
  29.3 1.4 %fusion = f32[2,2,512]{2,1,0:T(2,128)S(1)} fusion(f32[2,768,512,2]{2,1,3,0:T(8,128)S(1)} %get-tuple-element.23, f32[2,2,512]{2,1,0:T(2,128)S(1)} %broadcast_maximum_fusion, pred[512,768]{0,1:T(8,128)(4,1)S(1)} %fusion.11), kind=kLoop, calls=%fused_computation.3 | loop fusion | flops 6289408 | bytes 6701056 | tf_op jit(solution)/shard_map/reduce_sum | solution.py:421
  30.6 1.2 %copy-done.1 = f32[2,768,512,2]{2,1,3,0:T(8,128)} copy-done((f32[2,768,512,2]{2,1,3,0:T(8,128)}, f32[2,768,512,2]{2,1,3,0:T(8,128)S(1)}, u32[]{:S(2)}) %copy-start.1) | copy-done | bytes 6291480
  31.8 0.1 exponential_add_fusion
  31.9 0.1 copy.32
  32.1 4.7 %fusion.12 = bf16[2,64,2,512]{3,1,2,0:T(8,128)(2,1)S(1)} fusion(bf16[768,2,64,1]{0,2,3,1:T(8,128)(2,1)S(1)} %bitcast.57, f32[2,768,512,2]{2,1,3,0:T(8,128)} %copy-done.1, f32[2,2,512]{2,1,0:T(2,128)S(1)} %exponential_add_fusion, f32[2,2,512]{2,1,0:T(2,128)S(1)} %broadcast_maximum_fusion, pred[512,768]{0,1:T(8,128)(4,1)S(1)} %fusion.11), kind=kOutput, calls=%fused_computation.24 | convolution fusion | flops 209321984 | bytes 7159808 | tf_op jit(solution)/shard_map/hgqk,khd->qhgd/dot_general | solution.py:423
  36.8 2.1 %convolution_convert_fusion = bf16[512,2048]{1,0:T(8,128)(2,1)} fusion(bf16[512,256]{0,1:T(8,128)(2,1)S(1)} %bitcast.54, bf16[256,2048]{1,0:T(8,128)(2,1)S(1)} %copy-done), kind=kOutput, calls=%fused_computation.18 | convolution fusion | flops 537919488 | bytes 3407872 | tf_op jit(solution)/shard_map/dot_general | solution.py:427
  38.9 74.5 %shard_map.176 = (bf16[384,512]{1,0:T(8,128)(2,1)}, bf16[128,2048]{1,0:T(8,128)(2,1)}) custom-call(bf16[8,144,384]{2,1,0:T(8,128)(2,1)} %fusion.9.pick_ref, bf16[384,2048]{1,0:T(8,128)(2,1)} %fusion.7.normed_ref, bf16[2048,256]{1,0:T(8,128)(2,1)} %bitcast.51, bf16[2048,256]{1,0:T(8,128)(2,1)} %bitcast.52, bf16[256,2048]{1,0:T(8,128)(2,1)} %bitcast.53, ...), custom_call_target="tpu_custom_call" | custom-call | tf_op jit(solution)/shard_map/pallas_call | solution.py:456
  113.3 1.9 %copy.40 = bf16[128,2048]{1,0:T(8,128)(2,1)} copy(bf16[128,2048]{1,0:T(8,128)(2,1)} %get-tuple-element.30) | data formatting | bytes 1048576
  115.2 1.8 %copy.41 = bf16[384,512]{1,0:T(8,128)(2,1)} copy(bf16[384,512]{1,0:T(8,128)(2,1)} %get-tuple-element.31) | data formatting | bytes 786432
  (44 shorter events, 0.5 us)
Async XLA Ops:
  0.6 36.1 %copy-start = (bf16[256,2048]{1,0:T(8,128)(2,1)S(1)}, bf16[256,2048]{1,0:T(8,128)(2,1)}, u32[]{:S(2)}) copy-start(bf16[256,2048]{1,0:T(8,128)(2,1)} %param.25) | copy-start | bytes 3145732
  0.7 5.3 %copy-start.10 = (f32[64]{0:T(128)S(1)}, f32[64]{0:T(128)}, u32[]{:S(2)}) copy-start(f32[64]{0:T(128)} %param.23) | copy-start | bytes 772
  2.9 3.4 %copy-start.3 = (bf16[512,2048]{1,0:T(8,128)(2,1)S(1)}, bf16[512,2048]{1,0:T(8,128)(2,1)}, u32[]{:S(2)}) copy-start(bf16[512,2048]{1,0:T(8,128)(2,1)} %param.17) | copy-start | bytes 6291460
  2.9 3.4 %copy-start.11 = (f32[2048]{0:T(1024)S(1)}, f32[2048]{0:T(1024)}, u32[]{:S(2)}) copy-start(f32[2048]{0:T(1024)} %param.18) | copy-start | bytes 24580
  2.9 5.2 %copy-start.9 = (f32[512]{0:T(512)}, f32[512]{0:T(512)S(1)}, u32[]{:S(2)}) copy-start(f32[512]{0:T(512)S(1)} %add_rsqrt_fusion.2) | copy-start | bytes 6148
  8.8 18.0 %collective-permute-start = (bf16[2,128,128]{2,1,0:T(8,128)(2,1)}, bf16[2,128,128]{2,1,0:T(8,128)(2,1)}, u32[]{:S(2)}, u32[]{:S(2)}) collective-permute-start(bf16[2,128,128]{2,1,0:T(8,128)(2,1)} %get-tuple-element.12), channel_id=1, source_target_pairs={{0,4},{4,8},{8,12},{12,16},{16,20},{20,24},{24,28},{1,5},{5,9},{9,... | collective-permute-start | bytes 196616 | tf_op jit(solution)/shard_map/ppermute | solution.py:27
  14.3 12.5 %collective-permute-start.1 = (bf16[2,128,128]{2,1,0:T(8,128)(2,1)}, bf16[2,128,128]{2,1,0:T(8,128)(2,1)}, u32[]{:S(2)}, u32[]{:S(2)}) collective-permute-start(bf16[2,128,128]{2,1,0:T(8,128)(2,1)} %get-tuple-element.13), channel_id=1, source_target_pairs={{4,0},{8,4},{12,8},{16,12},{20,16},{24,20},{28,24},{5,1},{9,5},{13... | collective-permute-start | bytes 196616 | tf_op jit(solution)/shard_map/ppermute | solution.py:28
  16.3 3.2 %copy-start.4 = (s32[384,2]{0,1:T(2,128)S(1)}, s32[384,2]{0,1:T(2,128)}, u32[]{:S(2)}) copy-start(s32[384,2]{0,1:T(2,128)} %param.28) | copy-start | bytes 9220
  16.3 3.4 %copy-start.5 = (f32[384,2]{0,1:T(2,128)S(1)}, f32[384,2]{0,1:T(2,128)}, u32[]{:S(2)}) copy-start(f32[384,2]{0,1:T(2,128)} %param.30) | copy-start | bytes 9220
  18.5 5.5 %copy-start.2 = (bf16[384,2048]{1,0:T(8,128)(2,1)S(1)}, bf16[384,2048]{1,0:T(8,128)(2,1)}, u32[]{:S(2)}) copy-start(bf16[384,2048]{1,0:T(8,128)(2,1)} %param.26) | copy-start | bytes 4718596
  18.5 5.8 %copy-start.6 = (f32[2048]{0:T(1024)S(1)}, f32[2048]{0:T(1024)}, u32[]{:S(2)}) copy-start(f32[2048]{0:T(1024)} %param.27) | copy-start | bytes 24580
  21.6 4.3 %copy-start.7 = (pred[768]{0:T(1024)(128)(4,1)S(1)}, pred[768]{0:T(1024)(128)(4,1)}, u32[]{:S(2)}) copy-start(pred[768]{0:T(1024)(128)(4,1)} %get-tuple-element.26) | copy-start | bytes 2308
  21.6 4.3 %copy-start.8 = (pred[768]{0:T(1024)(128)(4,1)S(1)}, pred[768]{0:T(1024)(128)(4,1)}, u32[]{:S(2)}) copy-start(pred[768]{0:T(1024)(128)(4,1)} %get-tuple-element.27) | copy-start | bytes 2308
  21.6 5.1 %copy-start.12 = (f32[4]{0:T(128)S(1)}, f32[4]{0:T(128)}, u32[]{:S(2)}) copy-start(f32[4]{0:T(128)} %param.24) | copy-start | bytes 52
  29.2 2.7 %copy-start.1 = (f32[2,768,512,2]{2,1,3,0:T(8,128)}, f32[2,768,512,2]{2,1,3,0:T(8,128)S(1)}, u32[]{:S(2)}) copy-start(f32[2,768,512,2]{2,1,3,0:T(8,128)S(1)} %get-tuple-element.23) | copy-start | bytes 18874372
